TPU v7x, 256 devices: a whole 4x4x8 slice. The times are simulated.
256 devices in a mesh: sp: 64 (over z, x, core), tp: 4 (over y).
Axes of the slice: x: 4, y: 4, z: 8, core: 2. Of those that a mesh axis runs over, the one named last changes fastest.
Arguments:
- q_first: bfloat16 [12288, 512], P('sp', 'tp'), may hold values from -6 to 6
- k_first: bfloat16 [12288, 512], P('sp', 'tp'), may hold values from -6 to 6
- q_second: bfloat16 [12288, 512], P('sp', 'tp'), may hold values from -6 to 6
- k_second: bfloat16 [12288, 512], P('sp', 'tp'), may hold values from -6 to 6
- values: bfloat16 [12288, 1024], P('sp', 'tp'), may hold values from -6 to 6
- lambdas: float32 [8], P('tp'), may hold values from 0.3 to 0.8
- head_gain: float32 [128], replicated, may hold values from 0.1 to 1.9
- out_weight: bfloat16 [1024, 2048], P('tp'), may hold values from -0.1875 to 0.1875
- residual_in: bfloat16 [12288, 2048], P('sp'), may hold values from -6 to 6
- mix_gain: float32 [2048], replicated, may hold values from 0.1 to 1.9
- gate_weight: bfloat16 [2048, 5632], P('sp', 'tp'), may hold values from -0.125 to 0.125
- up_weight: bfloat16 [2048, 5632], P('sp', 'tp'), may hold values from -0.125 to 0.125
- gate_taps: float32 [3, 5632], P(None, 'tp'), may hold values from -3.5 to 3.5
- up_taps: float32 [3, 5632], P(None, 'tp'), may hold values from -3.5 to 3.5
- down_weight: bfloat16 [5632, 2048], P('tp'), may hold values from -0.078125 to 0.078125
Outputs:
- mixed: bfloat16 [12288, 2048], P(('sp', 'tp'))
All inputs are finite; a program needn't handle non-finite values.
Results may differ from a plain program's by a relative error of at most 0.017.
Values may be sent and summed in bfloat16 or wider, within the bound.
A program may use at most 128 MiB of HBM per device.

v0:
```python
import jax
import jax.numpy as jnp
from jax import lax
from jax.sharding import PartitionSpec as P

norm_eps = 1e-06
far_below = -1e30


def side_by_side(arrays, axis, dim, along):
    both = jnp.concatenate(arrays, axis=along)
    out, at, outs = (lax.all_gather(both, axis, axis=dim, tiled=True), 0, [])
    for a in arrays:
        outs.append(lax.slice_in_dim(out, at, at + a.shape[along], axis=along))
        at += a.shape[along]
    return tuple(outs)


def split_up(array, dim, devices):
    dims = array.shape
    blocks = array.reshape(*dims[:dim], devices, dims[dim] // devices, *dims[dim + 1 :])
    return jnp.moveaxis(blocks, dim, 0)


def sent_and_summed(array, axis, dim):
    blocks = split_up(array, dim, lax.axis_size(axis))
    arrived = lax.all_to_all(blocks, axis, split_axis=0, concat_axis=0, tiled=True)
    return arrived.astype(jnp.float32).sum(axis=0)


def passed_along(value, axis, steps):
    count = lax.axis_size(axis)
    initial, last = (max(0, -steps), min(count, count - steps))
    return lax.ppermute(value, axis, [(source, source + steps) for source in range(initial, last)])


def block_span(count, limit):
    return max((width for width in range(1, min(count, limit) + 1) if count % width == 0))


def update(peaks, totals, accum, scores, vals, visible):
    masked = jnp.where(visible, scores, far_below)
    new_peaks = jnp.maximum(peaks, jnp.max(masked, axis=-1))
    fade = jnp.exp(peaks - new_peaks)
    weights = jnp.where(visible, jnp.exp(masked - new_peaks[..., None]), 0.0)
    totals = totals * fade + jnp.sum(weights, axis=-1)
    accum = accum * fade.T[..., None] + jnp.einsum(
        "hqk,khv->qhv", weights.astype(jnp.bfloat16), vals, preferred_element_type=jnp.float32
    )
    return (new_peaks, totals, accum)


def rms_scale(field, gain):
    return field * lax.rsqrt(jnp.mean(field * field, axis=-1, keepdims=True) + norm_eps) * gain


def shards(
    q_first,
    k_first,
    q_second,
    k_second,
    values,
    lambdas,
    head_gain,
    out_weight,
    residual_in,
    mix_gain,
    gate_weight,
    up_weight,
    gate_taps,
    up_taps,
    down_weight,
):
    tok_rows = q_first.shape[0]
    head_count = lambdas.shape[0]
    head_dim = q_first.shape[1] // head_count
    value_dim = values.shape[1] // head_count
    part_rows = tok_rows // lax.axis_size("tp")
    tp_rank = lax.axis_index("tp")
    scale = head_dim ** (-0.5)
    query_pos = lax.axis_index("sp") * tok_rows + jnp.arange(tok_rows, dtype=jnp.int32)
    query_a = q_first.reshape(tok_rows, head_count, head_dim)
    query_b = q_second.reshape(tok_rows, head_count, head_dim)
    gate_full, up_full = side_by_side((gate_weight, up_weight), "sp", 0, 1)
    peaks_start = jnp.full((head_count, tok_rows), far_below, jnp.float32)
    totals_start = jnp.zeros((head_count, tok_rows), jnp.float32)
    accum_start = jnp.zeros((tok_rows, head_count, value_dim), jnp.float32)
    start = jnp.int32(0)
    keys_a, keys_b, vals = side_by_side((k_first, k_second, values), "sp", 0, 1)
    count = keys_a.shape[0]
    span = block_span(count, 2048)

    def step(index, inner):
        peaks_a, totals_a, accum_a, peaks_b, totals_b, accum_b = inner
        offset = index * span
        block_a = lax.dynamic_slice_in_dim(keys_a, offset, span, 0).reshape(
            span, head_count, head_dim
        )
        block_b = lax.dynamic_slice_in_dim(keys_b, offset, span, 0).reshape(
            span, head_count, head_dim
        )
        block_v = lax.dynamic_slice_in_dim(vals, offset, span, 0).reshape(
            span, head_count, value_dim
        )
        key_pos = start + offset + jnp.arange(span, dtype=jnp.int32)
        visible = (key_pos[None, :] <= query_pos[:, None])[None]
        scores_a = (
            jnp.einsum("qhd,khd->hqk", query_a, block_a, preferred_element_type=jnp.float32) * scale
        )
        scores_b = (
            jnp.einsum("qhd,khd->hqk", query_b, block_b, preferred_element_type=jnp.float32) * scale
        )
        peaks_a, totals_a, accum_a = update(peaks_a, totals_a, accum_a, scores_a, block_v, visible)
        peaks_b, totals_b, accum_b = update(peaks_b, totals_b, accum_b, scores_b, block_v, visible)
        return (peaks_a, totals_a, accum_a, peaks_b, totals_b, accum_b)

    carry = lax.fori_loop(
        0,
        count // span,
        step,
        (peaks_start, totals_start, accum_start, peaks_start, totals_start, accum_start),
    )
    first = carry[2] / carry[1].T[..., None]
    second = carry[5] / carry[4].T[..., None]
    diff_heads = first - lambdas[None, :, None] * second
    head_out = (
        rms_scale(diff_heads, head_gain)
        .astype(jnp.bfloat16)
        .reshape(tok_rows, head_count * value_dim)
    )
    attended = sent_and_summed(
        jnp.dot(head_out, out_weight, preferred_element_type=jnp.float32).astype(jnp.bfloat16),
        "tp",
        0,
    )
    own_rows = lax.dynamic_slice_in_dim(residual_in, tp_rank * part_rows, part_rows, 0)
    stream_rows = own_rows.astype(jnp.float32) + attended
    normed_part = rms_scale(stream_rows, mix_gain).astype(jnp.bfloat16)
    ffn_in = lax.all_gather(normed_part, "tp", axis=0, tiled=True)
    gate_pre = jnp.dot(ffn_in, gate_full, preferred_element_type=jnp.float32)
    up_pre = jnp.dot(ffn_in, up_full, preferred_element_type=jnp.float32)
    projected = jnp.stack((gate_pre.astype(jnp.bfloat16), up_pre.astype(jnp.bfloat16)))
    tap_count = gate_taps.shape[0]
    edge = passed_along(projected[:, tok_rows - (tap_count - 1) :], "sp", 1)
    padded = jnp.concatenate((edge, projected), axis=1).astype(jnp.float32)
    taps = jnp.stack((gate_taps, up_taps))
    convolved = taps[:, 0][:, None, :] * padded[:, 0:tok_rows]
    for offset in range(1, tap_count):
        convolved = convolved + taps[:, offset][:, None, :] * padded[:, offset : offset + tok_rows]
    hidden = (jax.nn.silu(convolved[0]) * convolved[1]).astype(jnp.bfloat16)
    down_rows = sent_and_summed(
        jnp.dot(hidden, down_weight, preferred_element_type=jnp.float32).astype(jnp.bfloat16),
        "tp",
        0,
    )
    return (stream_rows + down_rows).astype(jnp.bfloat16)


def solution(mesh):
    in_specs = (
        P("sp", "tp"),
        P("sp", "tp"),
        P("sp", "tp"),
        P("sp", "tp"),
        P("sp", "tp"),
        P("tp"),
        P(),
        P("tp", None),
        P("sp", None),
        P(),
        P("sp", "tp"),
        P("sp", "tp"),
        P(None, "tp"),
        P(None, "tp"),
        P("tp", None),
    )
    out_specs = P(("sp", "tp"), None)
    return jax.shard_map(shards, mesh=mesh, in_specs=in_specs, out_specs=out_specs, check_vma=False)
```

profile of v0, /device:TPU:8, one launch (start us, length us, event | category | flops | bytes accessed | tf_op | source)
XLA Modules:
  0.0 290.6 jit_solution(5387317274838956600)
XLA Ops:
  6.5 1.7 pad_maximum_fusion
  8.3 1.6 pad_maximum_fusion.1
  10.0 1.5 copy.32
  12.5 90.0 %all-gather.3.cloned.1.call-done = bf16[12288,512]{1,0:T(8,128)(2,1)} async-done(((bf16[192,512]{1,0:T(8,128)(2,1)}), bf16[12288,512]{1,0:T(8,128)(2,1)}) %all-gather.3.cloned.1.call-update) | async-done | bytes 12582928 | tf_op jit(solution)/shard_map/all_gather | solution.py:12
  102.5 5.4 %fusion.66 = (bf16[12288,128]{1,0:T(8,128)(2,1)}, bf16[12288,128]{1,0:T(8,128)(2,1)}) fusion(bf16[12288,512]{1,0:T(8,128)(2,1)} %all-gather.3.cloned.1.call-done), kind=kLoop, calls=%fused_computation.90 | loop fusion | bytes 12582912 | tf_op jit(solution)/shard_map/slice | solution.py:14
  107.9 3.3 %copy-done.2 = bf16[12288,512]{1,0:T(8,128)(2,1)S(1)} copy-done((bf16[12288,512]{1,0:T(8,128)(2,1)S(1)}, bf16[12288,512]{1,0:T(8,128)(2,1)}, u32[]{:S(2)}) %copy-start.2) | copy-done | bytes 12582936
  111.2 2.9 %slice.57 = bf16[12288,256]{1,0:T(8,128)(2,1)} slice(bf16[12288,512]{1,0:T(8,128)(2,1)S(1)} %copy-done.2), slice={[0:12288], [256:512]} | slice | bytes 12582912 | tf_op jit(solution)/shard_map/slice | solution.py:14
  114.1 104.1 %while.24 = (s32[]{:T(128)}, f32[2,192]{1,0:T(2,128)S(1)}, f32[2,192]{1,0:T(2,128)S(1)}, f32[192,2,128]{2,0,1:T(8,128)}, f32[2,192]{1,0:T(2,128)S(1)}, /*index=5...) while((s32[]{:T(128)}, f32[2,192]{1,0:T(2,128)S(1)}, ...), condition=%wide.region_5.6_spmd.clone, body=%wide.region_0.5_spmd.clone.sunk | while | flops 618830528 | bytes 48281516 | solution.py:117
  114.1 1.1 constant_dynamic-slice_fusion.7
  115.8 2.5 fusion.105
  118.9 1.3 constant_dynamic-slice_fusion.8
  120.9 3.4 %fusion.110 = f32[192,2,128]{2,0,1:T(8,128)} fusion(bf16[2048,2,128]{0,2,1:T(8,128)(2,1)S(1)} %bitcast.95, f32[2,192,2048]{2,1,0:T(8,128)} %get-tuple-element.437, f32[2,192]{1,0:T(2,128)S(1)} %get-tuple-element.485, pred[192,2048]{1,0:T(8,128)(4,1)S(1)} %broadcast_compare_fusion.2, f32[192,2,128]{2,0,1:T(8,128)} %get-tuple-element.470, ...), kind=kOutput, calls=%fused_computation.19.clone.1 | convolution fusion | flops 203833344 | bytes 4983809 | tf_op jit(solution)/shard_map/while/body/eval_jaxpr/hqk,khv->qhv/dot_general | solution.py:47
  124.3 1.1 constant_dynamic-slice_fusion.6
  125.6 1.8 fusion.103
  128.3 1.0 copy-done.1
  129.3 1.5 fusion.107
  131.4 1.1 constant_dynamic-slice_fusion.7
  133.1 2.5 fusion.105
  136.2 1.3 constant_dynamic-slice_fusion.8
  138.2 3.5 %fusion.110 = f32[192,2,128]{2,0,1:T(8,128)} fusion(bf16[2048,2,128]{0,2,1:T(8,128)(2,1)S(1)} %bitcast.95, f32[2,192,2048]{2,1,0:T(8,128)} %get-tuple-element.437, f32[2,192]{1,0:T(2,128)S(1)} %get-tuple-element.485, pred[192,2048]{1,0:T(8,128)(4,1)S(1)} %broadcast_compare_fusion.2, f32[192,2,128]{2,0,1:T(8,128)} %get-tuple-element.470, ...), kind=kOutput, calls=%fused_computation.19.clone.1 | convolution fusion | flops 203833344 | bytes 4983809 | tf_op jit(solution)/shard_map/while/body/eval_jaxpr/hqk,khv->qhv/dot_general | solution.py:47
  141.6 1.1 constant_dynamic-slice_fusion.6
  142.9 1.8 fusion.103
  146.6 1.5 fusion.107
  148.7 1.1 constant_dynamic-slice_fusion.7
  150.4 2.6 fusion.105
  153.5 1.3 constant_dynamic-slice_fusion.8
  155.5 3.4 %fusion.110 = f32[192,2,128]{2,0,1:T(8,128)} fusion(bf16[2048,2,128]{0,2,1:T(8,128)(2,1)S(1)} %bitcast.95, f32[2,192,2048]{2,1,0:T(8,128)} %get-tuple-element.437, f32[2,192]{1,0:T(2,128)S(1)} %get-tuple-element.485, pred[192,2048]{1,0:T(8,128)(4,1)S(1)} %broadcast_compare_fusion.2, f32[192,2,128]{2,0,1:T(8,128)} %get-tuple-element.470, ...), kind=kOutput, calls=%fused_computation.19.clone.1 | convolution fusion | flops 203833344 | bytes 4983809 | tf_op jit(solution)/shard_map/while/body/eval_jaxpr/hqk,khv->qhv/dot_general | solution.py:47
  158.9 1.1 constant_dynamic-slice_fusion.6
  160.2 1.8 fusion.103
  163.0 1.0 copy-done.1
  164.0 1.5 fusion.107
  166.1 1.1 constant_dynamic-slice_fusion.7
  167.7 2.5 fusion.105
  170.8 1.4 constant_dynamic-slice_fusion.8
  172.9 3.5 %fusion.110 = f32[192,2,128]{2,0,1:T(8,128)} fusion(bf16[2048,2,128]{0,2,1:T(8,128)(2,1)S(1)} %bitcast.95, f32[2,192,2048]{2,1,0:T(8,128)} %get-tuple-element.437, f32[2,192]{1,0:T(2,128)S(1)} %get-tuple-element.485, pred[192,2048]{1,0:T(8,128)(4,1)S(1)} %broadcast_compare_fusion.2, f32[192,2,128]{2,0,1:T(8,128)} %get-tuple-element.470, ...), kind=kOutput, calls=%fused_computation.19.clone.1 | convolution fusion | flops 203833344 | bytes 4983809 | tf_op jit(solution)/shard_map/while/body/eval_jaxpr/hqk,khv->qhv/dot_general | solution.py:47
  176.4 1.1 constant_dynamic-slice_fusion.6
  177.8 1.8 fusion.103
  180.5 1.0 copy-done.1
  181.5 1.5 fusion.107
  183.6 1.1 constant_dynamic-slice_fusion.7
  185.3 2.5 fusion.105
  188.4 1.3 constant_dynamic-slice_fusion.8
  190.4 3.4 %fusion.110 = f32[192,2,128]{2,0,1:T(8,128)} fusion(bf16[2048,2,128]{0,2,1:T(8,128)(2,1)S(1)} %bitcast.95, f32[2,192,2048]{2,1,0:T(8,128)} %get-tuple-element.437, f32[2,192]{1,0:T(2,128)S(1)} %get-tuple-element.485, pred[192,2048]{1,0:T(8,128)(4,1)S(1)} %broadcast_compare_fusion.2, f32[192,2,128]{2,0,1:T(8,128)} %get-tuple-element.470, ...), kind=kOutput, calls=%fused_computation.19.clone.1 | convolution fusion | flops 203833344 | bytes 4983809 | tf_op jit(solution)/shard_map/while/body/eval_jaxpr/hqk,khv->qhv/dot_general | solution.py:47
  193.9 1.1 constant_dynamic-slice_fusion.6
  195.2 1.8 fusion.103
  198.9 1.5 fusion.107
  201.0 1.1 constant_dynamic-slice_fusion.7
  202.6 2.5 fusion.105
  205.8 1.3 constant_dynamic-slice_fusion.8
  207.7 3.4 %fusion.110 = f32[192,2,128]{2,0,1:T(8,128)} fusion(bf16[2048,2,128]{0,2,1:T(8,128)(2,1)S(1)} %bitcast.95, f32[2,192,2048]{2,1,0:T(8,128)} %get-tuple-element.437, f32[2,192]{1,0:T(2,128)S(1)} %get-tuple-element.485, pred[192,2048]{1,0:T(8,128)(4,1)S(1)} %broadcast_compare_fusion.2, f32[192,2,128]{2,0,1:T(8,128)} %get-tuple-element.470, ...), kind=kOutput, calls=%fused_computation.19.clone.1 | convolution fusion | flops 203833344 | bytes 4983809 | tf_op jit(solution)/shard_map/while/body/eval_jaxpr/hqk,khv->qhv/dot_general | solution.py:47
  211.1 1.1 constant_dynamic-slice_fusion.6
  212.5 1.8 fusion.103
  216.1 1.5 fusion.107
  218.3 1.4 multiply_reduce_fusion.1
  219.7 2.0 convolution_convert_fusion.1
  221.7 4.8 %all-to-all-start = ((bf16[4,48,2048]{2,1,0:T(8,128)(2,1)}), bf16[4,48,2048]{2,1,0:T(8,128)(2,1)S(1)}, u32[]{:S(2)}, u32[]{:S(2)}) async-start(bf16[4,48,2048]{2,1,0:T(8,128)(2,1)} %bitcast.4), calls=%async_computation | async-start | bytes 1572864 | tf_op jit(solution)/shard_map/all_to_all | solution.py:27
  226.6 11.3 %all-to-all-done = bf16[4,48,2048]{2,1,0:T(8,128)(2,1)S(1)} async-done(((bf16[4,48,2048]{2,1,0:T(8,128)(2,1)}), bf16[4,48,2048]{2,1,0:T(8,128)(2,1)S(1)}, u32[]{:S(2)}, u32[]{:S(2)}) %all-to-all-start) | async-done | bytes 786464 | tf_op jit(solution)/shard_map/all_to_all | solution.py:27
  238.3 13.4 %all_gather.10 = bf16[192,2048]{1,0:T(8,128)(2,1)S(1)} all-gather(bf16[48,2048]{1,0:T(8,128)(2,1)S(1)} %multiply_convert_fusion), channel_id=1, replica_groups=mesh['sp'=64,'tp'=4] {'tp'}, dimensions={0}, use_global_device_ids=true | all-gather | bytes 983040 | tf_op jit(solution)/shard_map/all_gather | solution.py:139
  251.7 4.0 %fusion.46 = bf16[1,192,1408]{2,1,0:T(8,128)(2,1)S(1)} fusion(bf16[192,2048]{1,0:T(8,128)(2,1)S(1)} %all_gather.10, bf16[2048,2816]{1,0:T(8,128)(2,1)} %all-gather.5.cloned.1.call-done), kind=kOutput, calls=%fused_computation.51 | convolution fusion | flops 1107566592 | bytes 7094272 | tf_op jit(solution)/shard_map/dot_general | solution.py:141
  255.7 4.0 %fusion.49 = bf16[1,192,1408]{2,1,0:T(8,128)(2,1)S(1)} fusion(bf16[192,2048]{1,0:T(8,128)(2,1)S(1)} %all_gather.10, bf16[2048,2816]{1,0:T(8,128)(2,1)} %all-gather.5.cloned.1.call-done), kind=kOutput, calls=%fused_computation.52 | convolution fusion | flops 1107566592 | bytes 7094272 | tf_op jit(solution)/shard_map/dot_general | solution.py:140
  259.8 1.5 collective-permute-start
  262.8 1.3 slice-done
  264.6 1.5 convolution_convert_fusion
  266.1 16.8 %all_to_all.10 = bf16[4,48,2048]{2,1,0:T(8,128)(2,1)S(1)} all-to-all(bf16[4,48,2048]{2,1,0:T(8,128)(2,1)S(1)} %bitcast.99), channel_id=1, replica_groups=mesh['sp'=64,'tp'=4] {'tp'}, dimensions={0} | all-to-all | bytes 1572864 | tf_op jit(solution)/shard_map/all_to_all | solution.py:27
  (194 shorter events, 28.0 us)
Async XLA Ops:
  6.5 213.2 %copy-start = (bf16[256,2048]{1,0:T(8,128)(2,1)S(1)}, bf16[256,2048]{1,0:T(8,128)(2,1)}, u32[]{:S(2)}) copy-start(bf16[256,2048]{1,0:T(8,128)(2,1)} %param.24) | copy-start | bytes 3145732
  6.5 95.9 %all-gather.3.cloned.1.call-start = ((), (), s32[]{:S(2)}) async-start(), calls=%async_computation.2 | async-start | bytes 12779520 | tf_op jit(solution)/shard_map/all_gather | solution.py:12
  8.3 243.4 %all-gather.5.cloned.1.call-start = ((), (), s32[]{:S(2)}) async-start(), calls=%async_computation.3 | async-start | bytes 11714560 | tf_op jit(solution)/shard_map/all_gather | solution.py:12
  102.5 8.7 %copy-start.2 = (bf16[12288,512]{1,0:T(8,128)(2,1)S(1)}, bf16[12288,512]{1,0:T(8,128)(2,1)}, u32[]{:S(2)}) copy-start(bf16[12288,512]{1,0:T(8,128)(2,1)} %all-gather.3.cloned.1.call-done) | copy-start | bytes 37748740
  114.1 4.2 %copy-start.3 = (bf16[192,2,64]{0,2,1:T(8,128)(2,1)}, bf16[192,2,64]{0,2,1:T(8,128)(2,1)S(1)}, u32[]{:S(2)}) copy-start(bf16[192,2,64]{0,2,1:T(8,128)(2,1)S(1)} %get-tuple-element.492) | copy-start | bytes 147460 | tf_op jit(solution)/shard_map/while
  125.6 1.8 copy-start.6
  127.4 1.9 copy-start.1
  129.3 1.5 copy-start.7
  129.3 1.5 copy-start.8
  129.3 2.1 copy-start.4
  130.8 0.6 copy-start.9
  131.4 4.2 %copy-start.3 = (bf16[192,2,64]{0,2,1:T(8,128)(2,1)}, bf16[192,2,64]{0,2,1:T(8,128)(2,1)S(1)}, u32[]{:S(2)}) copy-start(bf16[192,2,64]{0,2,1:T(8,128)(2,1)S(1)} %get-tuple-element.492) | copy-start | bytes 147460 | tf_op jit(solution)/shard_map/while
  142.9 1.8 copy-start.6
  144.7 1.9 copy-start.1
  146.6 1.5 copy-start.7
  146.6 1.5 copy-start.8
  146.6 2.1 copy-start.4
  148.1 0.6 copy-start.9
  148.7 4.2 %copy-start.3 = (bf16[192,2,64]{0,2,1:T(8,128)(2,1)}, bf16[192,2,64]{0,2,1:T(8,128)(2,1)S(1)}, u32[]{:S(2)}) copy-start(bf16[192,2,64]{0,2,1:T(8,128)(2,1)S(1)} %get-tuple-element.492) | copy-start | bytes 147460 | tf_op jit(solution)/shard_map/while
  160.2 1.8 copy-start.6
  162.0 1.9 copy-start.1
  164.0 1.5 copy-start.7
  164.0 1.5 copy-start.8
  164.0 2.1 copy-start.4
  165.5 0.6 copy-start.9
  166.1 4.2 %copy-start.3 = (bf16[192,2,64]{0,2,1:T(8,128)(2,1)}, bf16[192,2,64]{0,2,1:T(8,128)(2,1)S(1)}, u32[]{:S(2)}) copy-start(bf16[192,2,64]{0,2,1:T(8,128)(2,1)S(1)} %get-tuple-element.492) | copy-start | bytes 147460 | tf_op jit(solution)/shard_map/while
  177.7 1.9 copy-start.6
  179.6 2.0 copy-start.1
  181.5 1.5 copy-start.7
  181.5 1.5 copy-start.8
  181.5 2.1 copy-start.4
  183.0 0.6 copy-start.9
  183.6 4.2 %copy-start.3 = (bf16[192,2,64]{0,2,1:T(8,128)(2,1)}, bf16[192,2,64]{0,2,1:T(8,128)(2,1)S(1)}, u32[]{:S(2)}) copy-start(bf16[192,2,64]{0,2,1:T(8,128)(2,1)S(1)} %get-tuple-element.492) | copy-start | bytes 147460 | tf_op jit(solution)/shard_map/while
  195.2 1.8 copy-start.6
  197.0 1.9 copy-start.1
  198.9 1.5 copy-start.7
  198.9 1.5 copy-start.8
  198.9 2.1 copy-start.4
  200.4 0.6 copy-start.9
  201.0 4.2 %copy-start.3 = (bf16[192,2,64]{0,2,1:T(8,128)(2,1)}, bf16[192,2,64]{0,2,1:T(8,128)(2,1)S(1)}, u32[]{:S(2)}) copy-start(bf16[192,2,64]{0,2,1:T(8,128)(2,1)S(1)} %get-tuple-element.492) | copy-start | bytes 147460 | tf_op jit(solution)/shard_map/while
  212.4 1.8 copy-start.6
  214.2 1.9 copy-start.1
  216.1 1.5 copy-start.7
  216.1 1.5 copy-start.8
  216.1 2.1 copy-start.4
  217.7 0.6 copy-start.9
  218.3 8.3 %copy-start.10 = (f32[3,1408]{1,0:T(4,128)S(1)}, f32[3,1408]{1,0:T(4,128)}, u32[]{:S(2)}) copy-start(f32[3,1408]{1,0:T(4,128)} %param.30) | copy-start | bytes 50692
  218.3 8.3 %copy-start.11 = (f32[3,1408]{1,0:T(4,128)S(1)}, f32[3,1408]{1,0:T(4,128)}, u32[]{:S(2)}) copy-start(f32[3,1408]{1,0:T(4,128)} %param.29) | copy-start | bytes 50692
  218.3 19.7 %copy-start.5 = (bf16[192,2048]{1,0:T(8,128)(2,1)S(1)}, bf16[192,2048]{1,0:T(8,128)(2,1)}, u32[]{:S(2)}) copy-start(bf16[192,2048]{1,0:T(8,128)(2,1)} %param.25) | copy-start | bytes 2359300
  218.3 19.9 %copy-start.12 = (f32[2048]{0:T(1024)S(1)}, f32[2048]{0:T(1024)}, u32[]{:S(2)}) copy-start(f32[2048]{0:T(1024)} %param.26) | copy-start | bytes 24580
  221.7 16.2 %all-to-all-start = ((bf16[4,48,2048]{2,1,0:T(8,128)(2,1)}), bf16[4,48,2048]{2,1,0:T(8,128)(2,1)S(1)}, u32[]{:S(2)}, u32[]{:S(2)}) async-start(bf16[4,48,2048]{2,1,0:T(8,128)(2,1)} %bitcast.4), calls=%async_computation | async-start | bytes 1572864 | tf_op jit(solution)/shard_map/all_to_all | solution.py:27
  259.8 2.1 collective-permute-start
  261.9 2.2 slice-start
  262.1 2.5 slice-start.1
Sparse Core Ops, SparseCore 0:
  10.1 92.3 all-gather.2
  105.2 84.6 all-gather.4
where the time goes:
time: 295 us; the launch traced here: 291 us
  waiting for transfers between devices  102 us (35%)
  matrix products  63.6 us (22%)
  local copies, waits for them, and re-layouts  52.9 us (18%)
  blocking collectives  30.2 us (10%)
  other arithmetic  21.3 us (7%)
  between operations  13.6 us (5%)
  starting transfers between devices  6.33 us (2%)
    all_gather x2, waiting for transfers between devices, side_by_side(): out, at, outs = (lax.all_gather(both, axis, axis=dim, tiled=True), 0, [])  90 us
    dot_general x12, matrix products, update(): jnp.einsum('hqk,khv->qhv', weights.astype(jnp.bfloat16), vals, preferred_...  26.1 us
    all_to_all x1, blocking collectives, sent_and_summed(): lax.all_to_all(blocks, axis, split_axis=0, concat_axis=0, tiled=True)  16.8 us
    dot_general x6, matrix products, step(): jnp.einsum('qhd,khd->hqk', query_b, block_b, preferred_element_type=jnp.f...  15.3 us
    all_gather x1, blocking collectives, shards(): ffn_in = lax.all_gather(normed_part, 'tp', axis=0, tiled=True)  13.4 us
    dynamic_slice x12, local copies, waits for them, and re-layouts, step(): lax.dynamic_slice_in_dim(vals, offset, span, 0)  11.8 us
    all_to_all x1, waiting for transfers between devices, sent_and_summed(): lax.all_to_all(blocks, axis, split_axis=0, concat_axis=0, tiled=True)  11.3 us
    dot_general x6, matrix products, step(): jnp.einsum('qhd,khd->hqk', query_a, block_a, preferred_element_type=jnp.f...  10.7 us
  transfers between devices with their start and end apart: 4, of which 3 were waited for; matrix products, arithmetic and copies ran while one was open for 38% of the time, Pallas kernels for 0%

commit v1 on v0

v1 whole, which is shorter than its diff:
```python
import functools

import jax
import jax.numpy as jnp
from jax import lax
from jax.experimental import pallas as pl
from jax.experimental.pallas import tpu as pltpu
from jax.sharding import PartitionSpec as P

MESH = pl.DeviceIdType.MESH
norm_eps = 1e-06
ROWS = 192
NX, NZ, NY = 4, 8, 4
DX = (2, 1, 3)
HIDE = -2e30
FLOOR = -1e30
f32, bf16 = jnp.float32, jnp.bfloat16


def rms_scale(field, gain):
    return field * lax.rsqrt(jnp.mean(field * field, axis=-1, keepdims=True) + norm_eps) * gain


def attention_kernel(
    qa, qb, ka, kb, va, gw, uw, lam, gain,
    head_out, wg_out, wu_out,
    q, kv, wg, wu, qz, m, l, acc, psend, precv, ssend, srecv,
    loc, bar_q, kvs, kvr, kds, kdr, wus, wur, wxs, wxr, wds, wdr, gxs, gxr, gzs, gzr, gds, gdr, pts, ptr, sts, str_,
):
    r = lax.axis_index("sp")
    y = lax.axis_index("tp")
    z, x, c = r // 8, (r // 2) % 4, r % 2

    def at(zz, xx, cc):
        return (lax.rem(zz + NZ, NZ) * 8 + lax.rem(xx + NX, NX) * 2 + cc, y)

    mate = (r + 1 - 2 * c, y)
    up_dev, down_dev = at(z + 1, x, c), at(z - 1, x, c)

    def rcopy(src, dst, ss, rs, dev):
        return pltpu.make_async_remote_copy(
            src_ref=src, dst_ref=dst, send_sem=ss, recv_sem=rs, device_id=dev, device_id_type=MESH
        )

    loads = [
        (qa, q.at[x, :, 0:128]),
        (qb, q.at[x, :, 128:256]),
        (ka, kv.at[z, c, :, 0:128]),
        (kb, kv.at[z, c, :, 128:256]),
        (va, kv.at[z, c, :, 256:512]),
        (gw, wg.at[z, x, c]),
        (uw, wu.at[z, x, c]),
    ]
    loads = [pltpu.make_async_copy(s, d, loc.at[i]) for i, (s, d) in enumerate(loads)]
    for d in loads:
        d.start()
    barrier = pltpu.get_barrier_semaphore()
    for dev in [up_dev, down_dev, mate] + [at(z, x + d, c) for d in DX]:
        pl.semaphore_signal(barrier, inc=1, device_id=dev, device_id_type=MESH)
    pl.semaphore_wait(barrier, 6)
    for d in loads:
        d.wait()

    def q_copy(i, slot):
        return rcopy(q.at[slot], q.at[slot], bar_q.at[0, i], bar_q.at[1, i], at(z, x + DX[i], c))

    plus_n, minus_n = 4 - c, 3 + c

    def z_ring(ref_at, sends, recvs):
        def plus(s):
            blk = lax.rem(z - s + 1 + NZ, NZ)
            return rcopy(ref_at(blk), ref_at(blk), sends.at[0, s - 1], recvs.at[0, s - 1], up_dev)

        def minus(s):
            blk = lax.rem(z + s - 1, NZ)
            return rcopy(ref_at(blk), ref_at(blk), sends.at[1, s - 1], recvs.at[1, s - 1], down_dev)

        def plus_in(s):
            blk = lax.rem(z - s + NZ, NZ)
            return rcopy(ref_at(blk), ref_at(blk), sends.at[0, s - 1], recvs.at[0, s - 1], up_dev)

        def minus_in(s):
            blk = lax.rem(z + s, NZ)
            return rcopy(ref_at(blk), ref_at(blk), sends.at[1, s - 1], recvs.at[1, s - 1], down_dev)

        return plus, minus, plus_in, minus_in

    def only(n, s, fn):
        if s <= 3:
            fn()
        elif s == 4:
            pl.when(n == 4)(fn)

    kv_ring = z_ring(lambda b: kv.at[b, c], kvs, kvr)
    wu_ring = z_ring(lambda b: wu.at[b, x, c], wus, wur)
    wg_ring = z_ring(lambda b: wg.at[b, :, c], gzs, gzr)

    def hand_blk(k):
        off = (0, -1, -2, -3, 1, 2, 3, 4)[k]
        return lax.rem(z + off + NZ, NZ)

    def kv_hand(k, lane):
        b = hand_blk(k)
        return rcopy(kv.at[b, lane], kv.at[b, lane], kds.at[k], kdr.at[k], mate)

    def wg_hand(k, lane):
        b = hand_blk(k)
        return rcopy(wg.at[b, :, lane], wg.at[b, :, lane], gds.at[k], gdr.at[k], mate)

    def wu_hand(k, lane):
        b = hand_blk(k)
        return rcopy(wu.at[b, :, lane], wu.at[b, :, lane], wds.at[k], wdr.at[k], mate)

    def wu_x(k, i, xx):
        b = hand_blk(k)
        return rcopy(wu.at[b, xx, c], wu.at[b, xx, c], wxs.at[k, i], wxr.at[k, i], at(z, x + DX[i], c))

    def wg_x(i, xx):
        return rcopy(wg.at[z, xx, c], wg.at[z, xx, c], gxs.at[i], gxr.at[i], at(z, x + DX[i], c))

    def from_x(i):
        return lax.rem(x - DX[i] + NX, NX)

    def ring_start(ring):
        ring[0](1).start()
        ring[1](1).start()

    def ring_step(ring, s, hand):
        def p():
            ring[2](s).wait_recv()
            only(plus_n, s + 1, lambda: ring[0](s + 1).start())
            if s < 4:
                hand(s)
            else:
                hand(7)

        def n():
            ring[3](s).wait_recv()
            only(minus_n, s + 1, lambda: ring[1](s + 1).start())
            if s < 4:
                hand(3 + s)
            else:
                hand(7)

        only(plus_n, s, p)
        only(minus_n, s, n)

    def ks(s):
        return (s, 3 + s) if s < 4 else (7,)

    for i in range(3):
        q_copy(i, x).start()
    ring_start(kv_ring)
    kv_hand(0, c).start()
    for i in range(3):
        wg_x(i, x).start()
    ring_start(wu_ring)
    for i in range(3):
        wu_x(0, i, x).start()

    m[...] = jnp.full_like(m, FLOOR)
    l[...] = jnp.zeros_like(l)
    acc[...] = jnp.zeros_like(acc)

    lane = lax.broadcasted_iota(jnp.int32, (ROWS, 128), 1)

    def prepare(slot):
        for half in range(2):
            block = q[slot, :, half * 128 : (half + 1) * 128] * bf16(0.125)
            zero = jnp.zeros_like(block)
            qz[half, slot, 0:ROWS] = jnp.where(lane < 64, block, zero)
            qz[half, slot, ROWS : 2 * ROWS] = jnp.where(lane < 64, zero, block)

    prepare(x)
    for i in range(3):
        q_copy(i, from_x(i)).wait_recv()
        prepare(from_x(i))

    def piece(pair, slot, masked):
        if masked:
            j = lax.broadcasted_iota(jnp.int32, (1, 768), 1)
            second = (j >= 384).astype(jnp.int32)
            core = ((j - 384 * second) >= 192).astype(jnp.int32)
            off = j - 384 * second - 192 * core
            key_pos = ((2 * pair + second) * 8 + x * 2 + core) * ROWS + off
            i = lax.broadcasted_iota(jnp.int32, (2 * ROWS, 1), 0)
            i = i - ROWS * (i >= ROWS).astype(jnp.int32)
            query_pos = (z * 8 + slot * 2 + c) * ROWS + i
            visible = key_pos <= query_pos
        for half in range(2):
            keys = kv[pl.ds(2 * pair, 2), :, :, half * 128 : (half + 1) * 128].reshape(768, 128)
            s = lax.dot_general(
                qz[half, slot], keys, (((1,), (1,)), ((), ())), preferred_element_type=f32
            )
            if masked:
                s = jnp.where(visible, s, HIDE)
            old = m[half, slot]
            new = jnp.maximum(old, jnp.max(s, axis=1, keepdims=True))
            fade = jnp.exp(old - new)
            m[half, slot] = new
            e = jnp.exp(s - new[:, 0:1])
            part = e[:, 0:128]
            for t in range(1, 6):
                part = part + e[:, t * 128 : (t + 1) * 128]
            l[half, slot] = l[half, slot] * fade + part
            eb = e.astype(bf16)
            for h in range(2):
                rows = slice(h * ROWS, (h + 1) * ROWS)
                vals = kv[pl.ds(2 * pair, 2), :, :, 256 + h * 128 : 384 + h * 128].reshape(768, 128)
                acc[half, slot, rows] = acc[half, slot, rows] * fade[rows] + jnp.dot(
                    eb[rows], vals, preferred_element_type=f32
                )

    own = z // 2
    odd = z % 2
    pairs = (
        own,
        lax.rem(own + jnp.where(odd == 1, 1, 3), 4),
        lax.rem(own + jnp.where(odd == 1, 3, 1), 4),
        lax.rem(own + 2, 4),
    )

    def sum_stats(slot):
        st = jnp.zeros((ROWS, 128), f32)
        for half in range(2):
            for h in range(2):
                rows = slice(h * ROWS, (h + 1) * ROWS)
                k = half * 2 + h
                st = jnp.where(lane == k, m[half, slot, rows], st)
                tot = jnp.sum(l[half, slot, rows], axis=1, keepdims=True)
                st = jnp.where(lane == 4 + k, tot, st)
        return st

    def p_copy(i):
        return rcopy(psend.at[i], precv.at[i], pts.at[i], ptr.at[i], (at(z, x + i_dx(i), c)))

    def s_copy(i):
        return rcopy(ssend.at[i], srecv.at[i], sts.at[i], str_.at[i], (at(z, x + i_dx(i), c)))

    def i_dx(i):
        return jnp.where(i == 0, 2, jnp.where(i == 1, 1, 3))

    wu_hand_waits = []
    for ci in range(4):
        s = ci + 1
        ring_step(kv_ring, s, lambda k: kv_hand(k, c).start())
        if ci == 0:
            kv_hand(0, 1 - c).wait_recv()
        for k in ks(s):
            kv_hand(k, 1 - c).wait_recv()
        pair = pairs[ci]
        if ci == 0:
            def body0(slot, carry):
                piece(pair, slot, True)
                return carry
            lax.fori_loop(0, 4, body0, 0)
        elif ci < 3:
            @pl.when(pair < own)
            def _():
                def body1(slot, carry):
                    piece(pair, slot, False)
                    return carry
                lax.fori_loop(0, 4, body1, 0)
        else:
            def body3(i, carry):
                slot = lax.rem(x + jnp.where(i == 3, 0, i_dx(i)), NX)

                @pl.when(pair < own)
                def _():
                    piece(pair, slot, False)

                @pl.when(i < 3)
                def _():
                    for half in range(2):
                        for h in range(2):
                            col = (half * 2 + h) * 128
                            psend[i, :, col : col + 128] = acc[
                                half, slot, h * ROWS : (h + 1) * ROWS
                            ].astype(bf16)
                    st = jnp.concatenate((sum_stats(slot), jnp.zeros((64, 128), f32)), axis=0)
                    ssend[i] = st.T[0:8]
                    p_copy(i).start()
                    s_copy(i).start()
                return carry
            lax.fori_loop(0, 4, body3, 0)

        ring_step(
            wu_ring, s,
            (lambda k: [wu_x(k, i, x).start() for i in range(3)]),
        )
        if ci == 0:
            for i in range(3):
                wg_x(i, from_x(i)).wait_recv()
            wg_hand(0, c).start()
        if ci == 1:
            for i in range(3):
                wu_x(0, i, from_x(i)).wait_recv()
            wu_hand(0, c).start()
            for k in ks(1):
                for i in range(3):
                    wu_x(k, i, from_x(i)).wait_recv()
                wu_hand(k, c).start()
        if ci == 2:
            ring_start(wg_ring)

    ring_step(wg_ring, 1, lambda k: wg_hand(k, c).start())

    def take(i):
        p_copy(i).wait_recv()
        s_copy(i).wait_recv()
        st = jnp.concatenate((srecv[i], jnp.zeros((120, 256), f32)), axis=0).T[0:ROWS]
        return st

    stats = [sum_stats(x)] + [take(i) for i in range(3)]
    for h in range(2):
        parts = []
        for half in range(2):
            k = half * 2 + h
            col = k * 128
            ms = [st[:, k : k + 1] for st in stats]
            ls = [st[:, 4 + k : 5 + k] for st in stats]
            top = functools.reduce(jnp.maximum, ms)
            ws = [jnp.exp(a - top) for a in ms]
            tot = sum(w * t for w, t in zip(ws, ls))
            out = acc[half, x, h * ROWS : (h + 1) * ROWS] * ws[0]
            for i in range(3):
                out = out + precv[i, :, col : col + 128].astype(f32) * ws[i + 1]
            parts.append(out / tot)
        diff = parts[0] - lam[h : h + 1, :] * parts[1]
        head_out[:, h * 128 : (h + 1) * 128] = rms_scale(diff, gain[...]).astype(bf16)

    def wu_finish(k):
        for i in range(3):
            wu_x(k, i, from_x(i)).wait_recv()
        wu_hand(k, c).start()

    for k in ks(2):
        wu_finish(k)
    ring_step(wg_ring, 2, lambda k: wg_hand(k, c).start())
    for k in ks(3):
        wu_finish(k)
    ring_step(wg_ring, 3, lambda k: wg_hand(k, c).start())
    wu_finish(7)
    ring_step(wg_ring, 4, lambda k: wg_hand(k, c).start())
    for k in range(8):
        wg_hand(k, 1 - c).wait_recv()
        wu_hand(k, 1 - c).wait_recv()

    a = pltpu.make_async_copy(wg, wg_out, loc.at[0])
    b = pltpu.make_async_copy(wu, wu_out, loc.at[1])
    a.start()
    b.start()

    for i in range(3):
        q_copy(i, x).wait_send()
        wg_x(i, x).wait_send()
        p_copy(i).wait_send()
        s_copy(i).wait_send()
    for ring in (kv_ring, wu_ring, wg_ring):
        for s in range(1, 5):
            only(plus_n, s, lambda: ring[0](s).wait_send())
            only(minus_n, s, lambda: ring[1](s).wait_send())
    for k in range(8):
        kv_hand(k, c).wait_send()
        wg_hand(k, c).wait_send()
        wu_hand(k, c).wait_send()
        for i in range(3):
            wu_x(k, i, x).wait_send()
    a.wait()
    b.wait()


def attention(qa, qb, ka, kb, va, gw, uw, lam, gain):
    ANY = pl.BlockSpec(memory_space=pl.ANY)
    VM = pl.BlockSpec(memory_space=pltpu.VMEM)
    ff = gw.shape[1]
    dma = pltpu.SemaphoreType.DMA
    return pl.pallas_call(
        attention_kernel,
        out_shape=(
            jax.ShapeDtypeStruct((ROWS, 256), bf16),
            jax.ShapeDtypeStruct((8, 4, 2, 32, ff), bf16),
            jax.ShapeDtypeStruct((8, 4, 2, 32, ff), bf16),
        ),
        in_specs=[ANY] * 7 + [VM, VM],
        out_specs=(VM, ANY, ANY),
        scratch_shapes=[
            pltpu.VMEM((4, ROWS, 256), bf16),
            pltpu.VMEM((8, 2, ROWS, 512), bf16),
            pltpu.VMEM((8, 4, 2, 32, ff), bf16),
            pltpu.VMEM((8, 4, 2, 32, ff), bf16),
            pltpu.VMEM((2, 4, 2 * ROWS, 128), bf16),
            pltpu.VMEM((2, 4, 2 * ROWS, 128), f32),
            pltpu.VMEM((2, 4, 2 * ROWS, 128), f32),
            pltpu.VMEM((2, 4, 2 * ROWS, 128), f32),
            pltpu.VMEM((3, ROWS, 512), bf16),
            pltpu.VMEM((3, ROWS, 512), bf16),
            pltpu.VMEM((3, 8, 256), f32),
            pltpu.VMEM((3, 8, 256), f32),
            dma((7,)),
            dma((2, 3)),
            dma((2, 4)),
            dma((2, 4)),
            dma((8,)),
            dma((8,)),
            dma((2, 4)),
            dma((2, 4)),
            dma((8, 3)),
            dma((8, 3)),
            dma((8,)),
            dma((8,)),
            dma((3,)),
            dma((3,)),
            dma((2, 4)),
            dma((2, 4)),
            dma((8,)),
            dma((8,)),
            dma((3,)),
            dma((3,)),
            dma((3,)),
            dma((3,)),
        ],
        compiler_params=pltpu.CompilerParams(
            collective_id=0, has_side_effects=True, vmem_limit_bytes=60 * 1024 * 1024
        ),
        name="attend",
    )(qa, qb, ka, kb, va, gw, uw, lam, gain)


def split_up(array, dim, devices):
    dims = array.shape
    blocks = array.reshape(*dims[:dim], devices, dims[dim] // devices, *dims[dim + 1 :])
    return jnp.moveaxis(blocks, dim, 0)


def sent_and_summed(array, axis, dim):
    blocks = split_up(array, dim, lax.axis_size(axis))
    arrived = lax.all_to_all(blocks, axis, split_axis=0, concat_axis=0, tiled=True)
    return arrived.astype(jnp.float32).sum(axis=0)


def passed_along(value, axis, steps):
    count = lax.axis_size(axis)
    initial, last = (max(0, -steps), min(count, count - steps))
    return lax.ppermute(value, axis, [(source, source + steps) for source in range(initial, last)])


def shards(
    q_first, k_first, q_second, k_second, values, lambdas, head_gain, out_weight, residual_in,
    mix_gain, gate_weight, up_weight, gate_taps, up_taps, down_weight,
):
    tok_rows = q_first.shape[0]
    part_rows = tok_rows // lax.axis_size("tp")
    tp_rank = lax.axis_index("tp")
    lam = jnp.broadcast_to(lambdas[:, None], (2, 128))
    head_out, gate_full, up_full = attention(
        q_first, q_second, k_first, k_second, values, gate_weight, up_weight, lam, head_gain[None]
    )
    gate_full = gate_full.reshape(2048, -1)
    up_full = up_full.reshape(2048, -1)
    attended = sent_and_summed(
        jnp.dot(head_out, out_weight, preferred_element_type=jnp.float32).astype(jnp.bfloat16),
        "tp",
        0,
    )
    own_rows = lax.dynamic_slice_in_dim(residual_in, tp_rank * part_rows, part_rows, 0)
    stream_rows = own_rows.astype(jnp.float32) + attended
    normed_part = rms_scale(stream_rows, mix_gain).astype(jnp.bfloat16)
    ffn_in = lax.all_gather(normed_part, "tp", axis=0, tiled=True)
    gate_pre = jnp.dot(ffn_in, gate_full, preferred_element_type=jnp.float32)
    up_pre = jnp.dot(ffn_in, up_full, preferred_element_type=jnp.float32)
    projected = jnp.stack((gate_pre.astype(jnp.bfloat16), up_pre.astype(jnp.bfloat16)))
    tap_count = gate_taps.shape[0]
    edge = passed_along(projected[:, tok_rows - (tap_count - 1) :], "sp", 1)
    padded = jnp.concatenate((edge, projected), axis=1).astype(jnp.float32)
    taps = jnp.stack((gate_taps, up_taps))
    convolved = taps[:, 0][:, None, :] * padded[:, 0:tok_rows]
    for offset in range(1, tap_count):
        convolved = convolved + taps[:, offset][:, None, :] * padded[:, offset : offset + tok_rows]
    hidden = (jax.nn.silu(convolved[0]) * convolved[1]).astype(jnp.bfloat16)
    down_rows = sent_and_summed(
        jnp.dot(hidden, down_weight, preferred_element_type=jnp.float32).astype(jnp.bfloat16),
        "tp",
        0,
    )
    return (stream_rows + down_rows).astype(jnp.bfloat16)


def solution(mesh):
    in_specs = (
        P("sp", "tp"), P("sp", "tp"), P("sp", "tp"), P("sp", "tp"), P("sp", "tp"),
        P("tp"), P(), P("tp", None), P("sp", None), P(),
        P("sp", "tp"), P("sp", "tp"), P(None, "tp"), P(None, "tp"), P("tp", None),
    )
    out_specs = P(("sp", "tp"), None)
    return jax.shard_map(shards, mesh=mesh, in_specs=in_specs, out_specs=out_specs, check_vma=False)
```

time: 295 us -> 151 us (0.51)
  waiting for transfers between devices: 102 us -> 12.6 us
  Pallas kernels: 0 us -> 84.3 us
  matrix products: 63.6 us -> 9.3 us
  local copies, waits for them, and re-layouts: 52.9 us -> 3.28 us
  other arithmetic: 21.3 us -> 2.19 us
  between operations: 13.6 us -> 0.15 us
    all_gather x2 -> x0, waiting for transfers between devices: 90 us -> none  [side_by_side(): out, at, outs = (lax.all_gather(both, axis, axis=dim, tiled=True), 0, [])]
    pallas_call x0 -> x1, Pallas kernels: none -> 84.3 us  [attention(): pl.pallas_call(attention_kernel, out_shape=(jax.ShapeDtypeStruct((ROWS, 2...]
    dot_general x24 -> x0, matrix products: 52.1 us -> none  [the longest x12 26.1 us: update(): jnp.einsum('hqk,khv->qhv', weights.astype(jnp.bfloat16), vals, preferred_...]
    dynamic_slice x36 -> x0, local copies, waits for them, and re-layouts: 27.5 us -> none  [the longest x12 11.8 us: step(): lax.dynamic_slice_in_dim(vals, offset, span, 0)]
    while x96 -> x0, local copies, waits for them, and re-layouts: 9.38 us -> none
    reduce_sum x6 -> x0, other arithmetic: 8.83 us -> none  [update(): totals = totals * fade + jnp.sum(weights, axis=-1)]
    slice x2 -> x0, local copies, waits for them, and re-layouts: 8.34 us -> none  [side_by_side(): outs.append(lax.slice_in_dim(out, at, at + a.shape[along], axis=along))]
    unnamed x20, local copies, waits for them, and re-layouts: 7.67 us -> 1.91 us
  transfers between devices with their start and end apart: 4 -> 2, of which waited for: 3 -> 2; matrix products, arithmetic and copies ran while one was open for 38% -> 0% of each run, Pallas kernels for 0% -> 0%
where the time goes in v1:
time: 151 us; the launch traced here: 149 us
  Pallas kernels  84.3 us (56%)
  blocking collectives  30.4 us (20%)
  waiting for transfers between devices  12.6 us (8%)
  matrix products  9.3 us (6%)
  starting transfers between devices  6.33 us (4%)
  local copies, waits for them, and re-layouts  3.28 us (2%)
  other arithmetic  2.19 us (1%)
    pallas_call x1, Pallas kernels, attention(): pl.pallas_call(attention_kernel, out_shape=(jax.ShapeDtypeStruct((ROWS, 2...  84.3 us
    all_to_all x1, blocking collectives, sent_and_summed(): lax.all_to_all(blocks, axis, split_axis=0, concat_axis=0, tiled=True)  17.3 us
    all_gather x1, blocking collectives, shards(): ffn_in = lax.all_gather(normed_part, 'tp', axis=0, tiled=True)  13.1 us
    all_to_all x1, waiting for transfers between devices, sent_and_summed(): lax.all_to_all(blocks, axis, split_axis=0, concat_axis=0, tiled=True)  11.8 us
    all_to_all x1, starting transfers between devices, sent_and_summed(): lax.all_to_all(blocks, axis, split_axis=0, concat_axis=0, tiled=True)  5.04 us
    dot_general x1, matrix products, shards(): gate_pre = jnp.dot(ffn_in, gate_full, preferred_element_type=jnp.float32)  4.21 us
  transfers between devices with their start and end apart: 2, of which 2 were waited for; matrix products, arithmetic and copies ran while one was open for 0% of the time, Pallas kernels for 0%

profile of v1, /device:TPU:8, one launch (start us, length us, event | category | flops | bytes accessed | tf_op | source)
XLA Modules:
  0.0 148.6 jit_solution(15244528521966811845)
XLA Ops:
  0.0 0.0 copy-start
  0.0 0.0 copy-start.3
  0.0 0.0 copy-start.2
  0.0 1.4 broadcast_in_dim.4.lam
  1.4 84.3 %attend.1 = (bf16[192,256]{1,0:T(8,128)(2,1)}, bf16[8,4,2,32,1408]{4,3,2,1,0:T(8,128)(2,1)}, bf16[8,4,2,32,1408]{4,3,2,1,0:T(8,128)(2,1)}) custom-call(bf16[192,128]{1,0:T(8,128)(2,1)} %qa.1, bf16[192,128]{1,0:T(8,128)(2,1)} %qb.1, bf16[192,128]{1,0:T(8,128)(2,1)} %ka.1, bf16[192,128]{1,0:T(8,128)(2,1)} %kb.1, bf16[192,256]{1,0:T(8,128)(2,1)} %va.1, ...), custom_call_target="tpu_custom_call" | custom-call | tf_op jit(solution)/shard_map/attend/pallas_call | solution.py:378
  85.7 0.0 copy-done
  85.7 0.0 copy-start.1
  85.8 2.2 %convolution_convert_fusion.3 = bf16[192,2048]{1,0:T(8,128)(2,1)} fusion(bf16[192,256]{1,0:T(8,128)(2,1)} %get-tuple-element.8, bf16[256,2048]{1,0:T(8,128)(2,1)S(1)} %copy-done), kind=kOutput, calls=%fused_computation.3 | convolution fusion | flops 201719808 | bytes 1933312 | tf_op jit(solution)/shard_map/dot_general | solution.py:462
  88.0 0.0 copy-start.4
  88.0 5.0 %all-to-all-start = ((bf16[4,48,2048]{2,1,0:T(8,128)(2,1)}), bf16[4,48,2048]{2,1,0:T(8,128)(2,1)S(1)}, u32[]{:S(2)}, u32[]{:S(2)}) async-start(bf16[4,48,2048]{2,1,0:T(8,128)(2,1)} %bitcast.1), calls=%async_computation | async-start | bytes 1572864 | tf_op jit(solution)/shard_map/all_to_all | solution.py:438
  93.0 0.0 copy-done.3
  93.0 0.0 copy-done.2
  93.1 11.8 %all-to-all-done = bf16[4,48,2048]{2,1,0:T(8,128)(2,1)S(1)} async-done(((bf16[4,48,2048]{2,1,0:T(8,128)(2,1)}), bf16[4,48,2048]{2,1,0:T(8,128)(2,1)S(1)}, u32[]{:S(2)}, u32[]{:S(2)}) %all-to-all-start) | async-done | bytes 786464 | tf_op jit(solution)/shard_map/all_to_all | solution.py:438
  104.9 0.0 slice-start.2
  104.9 0.1 convert_reduce_fusion.1
  105.0 0.0 copy-done.1
  105.0 0.2 multiply_reduce_fusion
  105.2 0.0 copy-done.4
  105.2 0.1 multiply_convert_fusion
  105.3 13.1 %all_gather.3 = bf16[192,2048]{1,0:T(8,128)(2,1)S(1)} all-gather(bf16[48,2048]{1,0:T(8,128)(2,1)S(1)} %multiply_convert_fusion), channel_id=1, replica_groups=mesh['sp'=64,'tp'=4] {'tp'}, dimensions={0}, use_global_device_ids=true | all-gather | bytes 983040 | tf_op jit(solution)/shard_map/all_gather | solution.py:469
  118.4 0.0 slice-start.3
  118.4 4.2 %fusion = bf16[1,192,1408]{2,1,0:T(8,128)(2,1)S(1)} fusion(bf16[192,2048]{1,0:T(8,128)(2,1)S(1)} %all_gather.3, bf16[2048,1408]{1,0:T(8,128)(2,1)} %bitcast.47), kind=kOutput, calls=%fused_computation.4 | convolution fusion | flops 1107566592 | bytes 7094272 | tf_op jit(solution)/shard_map/dot_general | solution.py:470
  122.7 0.0 slice-done.2
  122.7 0.0 slice-done.3
  122.7 1.4 fusion.1
  124.1 1.3 collective-permute-start
  125.5 0.8 collective-permute-done
  126.2 0.0 slice-start
  126.2 0.2 maximum_convert_fusion
  126.5 0.0 slice-start.1
  126.5 0.6 fusion.2
  127.1 1.3 slice-done
  128.4 0.5 slice-done.1
  129.0 1.5 convolution_convert_fusion
  130.4 17.3 %all_to_all.10 = bf16[4,48,2048]{2,1,0:T(8,128)(2,1)S(1)} all-to-all(bf16[4,48,2048]{2,1,0:T(8,128)(2,1)S(1)} %bitcast.37), channel_id=1, replica_groups=mesh['sp'=64,'tp'=4] {'tp'}, dimensions={0} | all-to-all | bytes 1572864 | tf_op jit(solution)/shard_map/all_to_all | solution.py:438
  147.7 0.1 convert_reduce_fusion
  147.8 0.8 add_convert_fusion
  (7 shorter events, 0.1 us)
Async XLA Ops:
  0.0 85.7 %copy-start = (bf16[256,2048]{1,0:T(8,128)(2,1)S(1)}, bf16[256,2048]{1,0:T(8,128)(2,1)}, u32[]{:S(2)}) copy-start(bf16[256,2048]{1,0:T(8,128)(2,1)} %param.22) | copy-start | bytes 3145732
  0.0 93.0 %copy-start.3 = (f32[3,1408]{1,0:T(4,128)S(1)}, f32[3,1408]{1,0:T(4,128)}, u32[]{:S(2)}) copy-start(f32[3,1408]{1,0:T(4,128)} %param.27) | copy-start | bytes 50692
  0.0 93.0 %copy-start.2 = (f32[3,1408]{1,0:T(4,128)S(1)}, f32[3,1408]{1,0:T(4,128)}, u32[]{:S(2)}) copy-start(f32[3,1408]{1,0:T(4,128)} %param.28) | copy-start | bytes 50692
  85.7 19.2 %copy-start.1 = (bf16[192,2048]{1,0:T(8,128)(2,1)S(1)}, bf16[192,2048]{1,0:T(8,128)(2,1)}, u32[]{:S(2)}) copy-start(bf16[192,2048]{1,0:T(8,128)(2,1)} %param.23) | copy-start | bytes 2359300
  88.0 17.2 %copy-start.4 = (f32[2048]{0:T(1024)S(1)}, f32[2048]{0:T(1024)}, u32[]{:S(2)}) copy-start(f32[2048]{0:T(1024)} %param.24) | copy-start | bytes 24580
  88.0 16.9 %all-to-all-start = ((bf16[4,48,2048]{2,1,0:T(8,128)(2,1)}), bf16[4,48,2048]{2,1,0:T(8,128)(2,1)S(1)}, u32[]{:S(2)}, u32[]{:S(2)}) async-start(bf16[4,48,2048]{2,1,0:T(8,128)(2,1)} %bitcast.1), calls=%async_computation | async-start | bytes 1572864 | tf_op jit(solution)/shard_map/all_to_all | solution.py:438
  104.9 17.8 %slice-start.2 = ((s8[5767168]{0:T(1024)(128)(4,1)}), s8[1572864]{0:T(1024)(128)(4,1)S(1)}, s32[]{:S(2)}) async-start(s8[5767168]{0:T(1024)(128)(4,1)} %bitcast.44), calls=%async_computation.4 | async-start | bytes 3145728
  118.4 4.2 %slice-start.3 = ((s8[5767168]{0:T(1024)(128)(4,1)}), s8[4194304]{0:T(1024)(128)(4,1)S(1)}, s32[]{:S(2)}) async-start(s8[5767168]{0:T(1024)(128)(4,1)} %bitcast.44), calls=%async_computation.5 | async-start | bytes 8388608
  124.1 2.1 %collective-permute-start = (bf16[2,2,1408]{2,1,0:T(2,128)(2,1)S(1)}, bf16[2,2,1408]{2,1,0:T(2,128)(2,1)S(1)}, u32[]{:S(2)}, u32[]{:S(2)}) collective-permute-start(bf16[2,2,1408]{2,1,0:T(2,128)(2,1)S(1)} %pad_maximum_fusion.2), channel_id=1, source_target_pairs={{0,4},{4,8},{8,12},{12,16},{16,20},{20,24},{24,28},{28,32},{32,36}... | collective-permute-start | bytes 33800 | tf_op jit(solution)/shard_map/ppermute | solution.py:445
  126.2 2.2 %slice-start = ((s8[5767168]{0:T(1024)(128)(4,1)}), s8[4194304]{0:T(1024)(128)(4,1)S(1)}, s32[]{:S(2)}) async-start(s8[5767168]{0:T(1024)(128)(4,1)} %bitcast.42), calls=%async_computation.2 | async-start | bytes 8388608
  126.5 2.5 %slice-start.1 = ((s8[5767168]{0:T(1024)(128)(4,1)}), s8[1572864]{0:T(1024)(128)(4,1)S(1)}, s32[]{:S(2)}) async-start(s8[5767168]{0:T(1024)(128)(4,1)} %bitcast.42), calls=%async_computation.3 | async-start | bytes 3145728

commit v2 on v1

--- a/solution.py
+++ b/solution.py
@@ -21,11 +21,13 @@
     return field * lax.rsqrt(jnp.mean(field * field, axis=-1, keepdims=True) + norm_eps) * gain
 
 
-def attention_kernel(
-    qa, qb, ka, kb, va, gw, uw, lam, gain,
-    head_out, wg_out, wu_out,
+def layer_kernel(
+    qa, qb, ka, kb, va, gw, uw, out_w, res_in, down_w, lam, gain, mix_gain, gate_taps, up_taps,
+    out,
     q, kv, wg, wu, qz, m, l, acc, psend, precv, ssend, srecv,
+    heads, ow, dw, res, stream, ffn, gate_pad, up_pad, hidden, edge_out, edge_in, part, drecv,
     loc, bar_q, kvs, kvr, kds, kdr, wus, wur, wxs, wxr, wds, wdr, gxs, gxr, gzs, gzr, gds, gdr, pts, ptr, sts, str_,
+    hys, hyr, oys, oyr, ods, odr, es, er, dys, dyr,
 ):
     r = lax.axis_index("sp")
     y = lax.axis_index("tp")
@@ -50,15 +52,21 @@
         (va, kv.at[z, c, :, 256:512]),
         (gw, wg.at[z, x, c]),
         (uw, wu.at[z, x, c]),
+        (out_w, ow.at[y]),
+        (res_in, res),
+        (down_w, dw),
     ]
     loads = [pltpu.make_async_copy(s, d, loc.at[i]) for i, (s, d) in enumerate(loads)]
     for d in loads:
         d.start()
     barrier = pltpu.get_barrier_semaphore()
-    for dev in [up_dev, down_dev, mate] + [at(z, x + d, c) for d in DX]:
+    across = [(r, lax.rem(y + d, NY)) for d in DX]
+    after, before = (lax.rem(r + 1, 64), y), (lax.rem(r + 63, 64), y)
+    greeted = [up_dev, down_dev, mate, after, before] + [at(z, x + d, c) for d in DX] + across
+    for dev in greeted:
         pl.semaphore_signal(barrier, inc=1, device_id=dev, device_id_type=MESH)
-    pl.semaphore_wait(barrier, 6)
-    for d in loads:
+    pl.semaphore_wait(barrier, len(greeted))
+    for d in loads[:5]:
         d.wait()
 
     def q_copy(i, slot):
@@ -148,19 +156,43 @@
     def ks(s):
         return (s, 3 + s) if s < 4 else (7,)
 
+    def from_y(i):
+        return lax.rem(y - DX[i] + NY, NY)
+
+    half_cols = ow.shape[2] // 2
+
+    def ow_y(i, yy):
+        ref = ow.at[yy, :, pl.ds(pl.multiple_of(c * half_cols, 128), half_cols)]
+        return rcopy(ref, ref, oys.at[i], oyr.at[i], across[i])
+
+    def ow_hand(i, lane):
+        ref = ow.at[from_y(i), :, pl.ds(pl.multiple_of(lane * half_cols, 128), half_cols)]
+        return rcopy(ref, ref, ods.at[i], odr.at[i], mate)
+
+    def heads_y(i, yy):
+        return rcopy(heads.at[yy], heads.at[yy], hys.at[i], hyr.at[i], across[i])
+
+    def edge_copy():
+        return rcopy(edge_out, edge_in, es, er, after)
+
+    def down_y(i, n):
+        return rcopy(
+            part.at[n, across[i][1]], drecv.at[i, n], dys.at[i, n], dyr.at[i, n], across[i]
+        )
+
     for i in range(3):
         q_copy(i, x).start()
     ring_start(kv_ring)
     kv_hand(0, c).start()
+    for d in loads[5:8]:
+        d.wait()
+    for i in range(3):
+        ow_y(i, y).start()
     for i in range(3):
         wg_x(i, x).start()
     ring_start(wu_ring)
     for i in range(3):
         wu_x(0, i, x).start()
-
-    m[...] = jnp.full_like(m, FLOOR)
-    l[...] = jnp.zeros_like(l)
-    acc[...] = jnp.zeros_like(acc)
 
     lane = lax.broadcasted_iota(jnp.int32, (ROWS, 128), 1)
 
@@ -194,22 +226,29 @@
             )
             if masked:
                 s = jnp.where(visible, s, HIDE)
-            old = m[half, slot]
-            new = jnp.maximum(old, jnp.max(s, axis=1, keepdims=True))
-            fade = jnp.exp(old - new)
+            if masked:
+                new = jnp.broadcast_to(
+                    jnp.maximum(jnp.max(s, axis=1, keepdims=True), FLOOR), (2 * ROWS, 128)
+                )
+            else:
+                old = m[half, slot]
+                new = jnp.maximum(old, jnp.max(s, axis=1, keepdims=True))
+                fade = jnp.exp(old - new)
             m[half, slot] = new
             e = jnp.exp(s - new[:, 0:1])
-            part = e[:, 0:128]
+            part_sum = e[:, 0:128]
             for t in range(1, 6):
-                part = part + e[:, t * 128 : (t + 1) * 128]
-            l[half, slot] = l[half, slot] * fade + part
+                part_sum = part_sum + e[:, t * 128 : (t + 1) * 128]
+            l[half, slot] = part_sum if masked else l[half, slot] * fade + part_sum
             eb = e.astype(bf16)
             for h in range(2):
                 rows = slice(h * ROWS, (h + 1) * ROWS)
                 vals = kv[pl.ds(2 * pair, 2), :, :, 256 + h * 128 : 384 + h * 128].reshape(768, 128)
-                acc[half, slot, rows] = acc[half, slot, rows] * fade[rows] + jnp.dot(
-                    eb[rows], vals, preferred_element_type=f32
-                )
+                more = jnp.dot(eb[rows], vals, preferred_element_type=f32)
+                if masked:
+                    acc[half, slot, rows] = more
+                else:
+                    acc[half, slot, rows] = acc[half, slot, rows] * fade[rows] + more
 
     own = z // 2
     odd = z % 2
@@ -302,6 +341,9 @@
                 wu_hand(k, c).start()
         if ci == 2:
             ring_start(wg_ring)
+            for i in range(3):
+                ow_y(i, from_y(i)).wait_recv()
+                ow_hand(i, c).start()
 
     ring_step(wg_ring, 1, lambda k: wg_hand(k, c).start())
 
@@ -322,12 +364,15 @@
             top = functools.reduce(jnp.maximum, ms)
             ws = [jnp.exp(a - top) for a in ms]
             tot = sum(w * t for w, t in zip(ws, ls))
-            out = acc[half, x, h * ROWS : (h + 1) * ROWS] * ws[0]
+            joined = acc[half, x, h * ROWS : (h + 1) * ROWS] * ws[0]
             for i in range(3):
-                out = out + precv[i, :, col : col + 128].astype(f32) * ws[i + 1]
-            parts.append(out / tot)
-        diff = parts[0] - lam[h : h + 1, :] * parts[1]
-        head_out[:, h * 128 : (h + 1) * 128] = rms_scale(diff, gain[...]).astype(bf16)
+                joined = joined + precv[i, :, col : col + 128].astype(f32) * ws[i + 1]
+            parts.append(joined / tot)
+        diff = parts[0] - lam[h] * parts[1]
+        heads[y, :, h * 128 : (h + 1) * 128] = rms_scale(diff, gain[...]).astype(bf16)
+
+    for i in range(3):
+        heads_y(i, y).start()
 
     def wu_finish(k):
         for i in range(3):
@@ -337,25 +382,89 @@
     for k in ks(2):
         wu_finish(k)
     ring_step(wg_ring, 2, lambda k: wg_hand(k, c).start())
+
+    loads[8].wait()
+    loads[9].wait()
+    for i in range(3):
+        ow_hand(i, 1 - c).wait_recv()
+    for i in range(3):
+        heads_y(i, from_y(i)).wait_recv()
+    width = stream.shape[2]
+    for n in range(0, width, 512):
+        cols = slice(n, n + 512)
+        total = res[:, cols].astype(f32)
+        for yy in range(NY):
+            total = total + jnp.dot(heads[yy], ow[yy, :, cols], preferred_element_type=f32)
+        stream[:, :, cols] = total.reshape(NY, ROWS // NY, 512)
+    rows = stream[...].reshape(ROWS, width)
+    ffn[...] = rms_scale(rows, mix_gain[...]).astype(bf16)
+
     for k in ks(3):
         wu_finish(k)
     ring_step(wg_ring, 3, lambda k: wg_hand(k, c).start())
     wu_finish(7)
     ring_step(wg_ring, 4, lambda k: wg_hand(k, c).start())
     for k in range(8):
+        wu_hand(k, 1 - c).wait_recv()
+    ff = hidden.shape[1]
+    for n in range(0, ff, 256):
+        cols = slice(n, min(n + 256, ff))
+        w = wu[:, :, :, :, cols].reshape(width, -1)
+        pre = jnp.dot(ffn[...], w, preferred_element_type=f32).astype(bf16).astype(f32)
+        up_pad[8 : 8 + ROWS, cols] = pre
+    for k in range(8):
         wg_hand(k, 1 - c).wait_recv()
-        wu_hand(k, 1 - c).wait_recv()
-
-    a = pltpu.make_async_copy(wg, wg_out, loc.at[0])
-    b = pltpu.make_async_copy(wu, wu_out, loc.at[1])
-    a.start()
-    b.start()
-
+    for n in range(0, ff, 256):
+        cols = slice(n, min(n + 256, ff))
+        w = wg[:, :, :, :, cols].reshape(width, -1)
+        pre = jnp.dot(ffn[...], w, preferred_element_type=f32).astype(bf16).astype(f32)
+        gate_pad[8 : 8 + ROWS, cols] = pre
+    edge_out[0] = gate_pad[6 + ROWS : 8 + ROWS, :]
+    edge_out[1] = up_pad[6 + ROWS : 8 + ROWS, :]
+    edge_copy().start()
+
+    def mix(top, size):
+        for n in range(0, ff, 128):
+            cols = slice(n, n + 128)
+            conv = []
+            for pad, taps in ((gate_pad, gate_taps), (up_pad, up_taps)):
+                v = taps[0:1, cols] * pad[6 + top : 6 + top + size, cols]
+                v = v + taps[1:2, cols] * pad[7 + top : 7 + top + size, cols]
+                v = v + taps[2:3, cols] * pad[8 + top : 8 + top + size, cols]
+                conv.append(v)
+            hidden[top : top + size, cols] = (jax.nn.silu(conv[0]) * conv[1]).astype(bf16)
+
+    mix(16, ROWS - 16)
+    edge_copy().wait_recv()
+    gate_pad[6:8, :] = jnp.where(r == 0, 0.0, edge_in[0])
+    up_pad[6:8, :] = jnp.where(r == 0, 0.0, edge_in[1])
+    mix(0, 16)
+
+    for n in range(NY):
+        cols = slice(n * 512, (n + 1) * 512)
+        down = jnp.dot(hidden[...], dw[:, cols], preferred_element_type=f32)
+        part[n] = down.astype(bf16).reshape(NY, ROWS // NY, 512)
+        for i in range(3):
+            down_y(i, n).start()
+    for n in range(NY):
+        cols = slice(n * 512, (n + 1) * 512)
+        total = stream[y, :, cols] + part[n, y].astype(f32)
+        for i in range(3):
+            down_y(i, n).wait_recv()
+            total = total + drecv[i, n].astype(f32)
+        out[:, cols] = total.astype(bf16)
+
+    edge_copy().wait_send()
     for i in range(3):
         q_copy(i, x).wait_send()
         wg_x(i, x).wait_send()
         p_copy(i).wait_send()
         s_copy(i).wait_send()
+        ow_y(i, y).wait_send()
+        ow_hand(i, c).wait_send()
+        heads_y(i, y).wait_send()
+        for n in range(NY):
+            down_y(i, n).wait_send()
     for ring in (kv_ring, wu_ring, wg_ring):
         for s in range(1, 5):
             only(plus_n, s, lambda: ring[0](s).wait_send())
@@ -366,24 +475,22 @@
         wu_hand(k, c).wait_send()
         for i in range(3):
             wu_x(k, i, x).wait_send()
-    a.wait()
-    b.wait()
-
-
-def attention(qa, qb, ka, kb, va, gw, uw, lam, gain):
+
+
+def layer(*args):
     ANY = pl.BlockSpec(memory_space=pl.ANY)
     VM = pl.BlockSpec(memory_space=pltpu.VMEM)
-    ff = gw.shape[1]
+    SM = pl.BlockSpec(memory_space=pltpu.SMEM)
+    ff, width = args[5].shape[1], args[8].shape[1]
     dma = pltpu.SemaphoreType.DMA
+    sems = [(10,), (2, 3), (2, 4), (2, 4), (8,), (8,), (2, 4), (2, 4), (8, 3), (8, 3), (8,), (8,)]
+    sems += [(3,), (3,), (2, 4), (2, 4), (8,), (8,), (3,), (3,), (3,), (3,)]
+    sems += [(3,), (3,), (3,), (3,), (3,), (3,), None, None, (3, 4), (3, 4)]
     return pl.pallas_call(
-        attention_kernel,
-        out_shape=(
-            jax.ShapeDtypeStruct((ROWS, 256), bf16),
-            jax.ShapeDtypeStruct((8, 4, 2, 32, ff), bf16),
-            jax.ShapeDtypeStruct((8, 4, 2, 32, ff), bf16),
-        ),
-        in_specs=[ANY] * 7 + [VM, VM],
-        out_specs=(VM, ANY, ANY),
+        layer_kernel,
+        out_shape=jax.ShapeDtypeStruct((ROWS // NY, width), bf16),
+        in_specs=[ANY] * 10 + [SM] + [VM] * 4,
+        out_specs=VM,
         scratch_shapes=[
             pltpu.VMEM((4, ROWS, 256), bf16),
             pltpu.VMEM((8, 2, ROWS, 512), bf16),
@@ -397,93 +504,35 @@
             pltpu.VMEM((3, ROWS, 512), bf16),
             pltpu.VMEM((3, 8, 256), f32),
             pltpu.VMEM((3, 8, 256), f32),
-            dma((7,)),
-            dma((2, 3)),
-            dma((2, 4)),
-            dma((2, 4)),
-            dma((8,)),
-            dma((8,)),
-            dma((2, 4)),
-            dma((2, 4)),
-            dma((8, 3)),
-            dma((8, 3)),
-            dma((8,)),
-            dma((8,)),
-            dma((3,)),
-            dma((3,)),
-            dma((2, 4)),
-            dma((2, 4)),
-            dma((8,)),
-            dma((8,)),
-            dma((3,)),
-            dma((3,)),
-            dma((3,)),
-            dma((3,)),
-        ],
+            pltpu.VMEM((NY, ROWS, 256), bf16),
+            pltpu.VMEM((NY, 256, width), bf16),
+            pltpu.VMEM((ff, width), bf16),
+            pltpu.VMEM((ROWS, width), bf16),
+            pltpu.VMEM((NY, ROWS // NY, width), f32),
+            pltpu.VMEM((ROWS, width), bf16),
+            pltpu.VMEM((8 + ROWS, ff), f32),
+            pltpu.VMEM((8 + ROWS, ff), f32),
+            pltpu.VMEM((ROWS, ff), bf16),
+            pltpu.VMEM((2, 2, ff), f32),
+            pltpu.VMEM((2, 2, ff), f32),
+            pltpu.VMEM((NY, NY, ROWS // NY, 512), bf16),
+            pltpu.VMEM((3, NY, ROWS // NY, 512), bf16),
+        ] + [dma if s is None else dma(s) for s in sems],
         compiler_params=pltpu.CompilerParams(
-            collective_id=0, has_side_effects=True, vmem_limit_bytes=60 * 1024 * 1024
+            collective_id=0, has_side_effects=True, vmem_limit_bytes=63 * 1024 * 1024
         ),
-        name="attend",
-    )(qa, qb, ka, kb, va, gw, uw, lam, gain)
-
-
-def split_up(array, dim, devices):
-    dims = array.shape
-    blocks = array.reshape(*dims[:dim], devices, dims[dim] // devices, *dims[dim + 1 :])
-    return jnp.moveaxis(blocks, dim, 0)
-
-
-def sent_and_summed(array, axis, dim):
-    blocks = split_up(array, dim, lax.axis_size(axis))
-    arrived = lax.all_to_all(blocks, axis, split_axis=0, concat_axis=0, tiled=True)
-    return arrived.astype(jnp.float32).sum(axis=0)
-
-
-def passed_along(value, axis, steps):
-    count = lax.axis_size(axis)
-    initial, last = (max(0, -steps), min(count, count - steps))
-    return lax.ppermute(value, axis, [(source, source + steps) for source in range(initial, last)])
+        name="layer",
+    )(*args)
 
 
 def shards(
     q_first, k_first, q_second, k_second, values, lambdas, head_gain, out_weight, residual_in,
     mix_gain, gate_weight, up_weight, gate_taps, up_taps, down_weight,
 ):
-    tok_rows = q_first.shape[0]
-    part_rows = tok_rows // lax.axis_size("tp")
-    tp_rank = lax.axis_index("tp")
-    lam = jnp.broadcast_to(lambdas[:, None], (2, 128))
-    head_out, gate_full, up_full = attention(
-        q_first, q_second, k_first, k_second, values, gate_weight, up_weight, lam, head_gain[None]
+    return layer(
+        q_first, q_second, k_first, k_second, values, gate_weight, up_weight, out_weight,
+        residual_in, down_weight, lambdas, head_gain[None], mix_gain[None], gate_taps, up_taps,
     )
-    gate_full = gate_full.reshape(2048, -1)
-    up_full = up_full.reshape(2048, -1)
-    attended = sent_and_summed(
-        jnp.dot(head_out, out_weight, preferred_element_type=jnp.float32).astype(jnp.bfloat16),
-        "tp",
-        0,
-    )
-    own_rows = lax.dynamic_slice_in_dim(residual_in, tp_rank * part_rows, part_rows, 0)
-    stream_rows = own_rows.astype(jnp.float32) + attended
-    normed_part = rms_scale(stream_rows, mix_gain).astype(jnp.bfloat16)
-    ffn_in = lax.all_gather(normed_part, "tp", axis=0, tiled=True)
-    gate_pre = jnp.dot(ffn_in, gate_full, preferred_element_type=jnp.float32)
-    up_pre = jnp.dot(ffn_in, up_full, preferred_element_type=jnp.float32)
-    projected = jnp.stack((gate_pre.astype(jnp.bfloat16), up_pre.astype(jnp.bfloat16)))
-    tap_count = gate_taps.shape[0]
-    edge = passed_along(projected[:, tok_rows - (tap_count - 1) :], "sp", 1)
-    padded = jnp.concatenate((edge, projected), axis=1).astype(jnp.float32)
-    taps = jnp.stack((gate_taps, up_taps))
-    convolved = taps[:, 0][:, None, :] * padded[:, 0:tok_rows]
-    for offset in range(1, tap_count):
-        convolved = convolved + taps[:, offset][:, None, :] * padded[:, offset : offset + tok_rows]
-    hidden = (jax.nn.silu(convolved[0]) * convolved[1]).astype(jnp.bfloat16)
-    down_rows = sent_and_summed(
-        jnp.dot(hidden, down_weight, preferred_element_type=jnp.float32).astype(jnp.bfloat16),
-        "tp",
-        0,
-    )
-    return (stream_rows + down_rows).astype(jnp.bfloat16)
 
 
 def solution(mesh):

time: 151 us -> 97.9 us (0.65); the launches traced: 149 us -> 97.5 us
  blocking collectives: 30.4 us -> 0 us
  waiting for transfers between devices: 12.6 us -> 0 us
  Pallas kernels: 84.3 us -> 95.8 us
  matrix products: 9.3 us -> 0 us
  starting transfers between devices: 6.33 us -> 0 us
  other arithmetic: 2.19 us -> 0 us
  local copies, waits for them, and re-layouts: 3.28 us -> 1.62 us
    all_to_all x1 -> x0, blocking collectives: 17.3 us -> none  [sent_and_summed(): lax.all_to_all(blocks, axis, split_axis=0, concat_axis=0, tiled=True)]
    all_gather x1 -> x0, blocking collectives: 13.1 us -> none  [shards(): ffn_in = lax.all_gather(normed_part, 'tp', axis=0, tiled=True)]
    all_to_all x1 -> x0, waiting for transfers between devices: 11.8 us -> none  [sent_and_summed(): lax.all_to_all(blocks, axis, split_axis=0, concat_axis=0, tiled=True)]
    pallas_call x1, Pallas kernels: 84.3 us -> 95.8 us  [layer(): pl.pallas_call(layer_kernel, out_shape=jax.ShapeDtypeStruct((ROWS // NY,...]
    dot_general x4 -> x0, matrix products: 9.3 us -> none  [the longest x1 4.21 us: shards(): gate_pre = jnp.dot(ffn_in, gate_full, preferred_element_type=jnp.float32)]
    all_to_all x1 -> x0, starting transfers between devices: 5.04 us -> none  [sent_and_summed(): lax.all_to_all(blocks, axis, split_axis=0, concat_axis=0, tiled=True)]
  transfers between devices with their start and end apart: 2 -> 0, of which waited for: 2 -> 0; matrix products, arithmetic and copies ran while one was open for 0% -> 0% of each run, Pallas kernels for 0% -> 0%
where the time goes in v2:
time: 97.9 us; the launch traced here: 97.5 us
  Pallas kernels  95.8 us (98%)
  local copies, waits for them, and re-layouts  1.62 us (2%)
    pallas_call x1, Pallas kernels, layer(): pl.pallas_call(layer_kernel, out_shape=jax.ShapeDtypeStruct((ROWS // NY,...  95.8 us

profile of v2, /device:TPU:8, one launch (start us, length us, event | category | flops | bytes accessed | tf_op | source)
XLA Modules:
  0.0 97.5 jit_solution(6843181194509297354)
XLA Ops:
  0.0 95.8 %layer.1 = bf16[48,2048]{1,0:T(8,128)(2,1)} custom-call(bf16[192,128]{1,0:T(8,128)(2,1)} %qa.1, bf16[192,128]{1,0:T(8,128)(2,1)} %qb.1, bf16[192,128]{1,0:T(8,128)(2,1)} %ka.1, bf16[192,128]{1,0:T(8,128)(2,1)} %kb.1, bf16[192,256]{1,0:T(8,128)(2,1)} %va.1, bf16[32,1408]{1,0:T(8,128)(2,1)} %gw.1, bf16[32,1408]{1,0:T(8,128)(2,1)} %uw.1, ...), custom_call_target="tpu_custom_call" | custom-call | tf_op jit(solution)/shard_map/layer/pallas_call | solution.py:489
  95.8 1.6 %copy.17 = bf16[48,2048]{1,0:T(8,128)(2,1)} copy(bf16[48,2048]{1,0:T(8,128)(2,1)} %layer.1) | data formatting | bytes 393216

commit v3 on v2

--- a/solution.py
+++ b/solution.py
@@ -101,7 +101,17 @@
 
     kv_ring = z_ring(lambda b: kv.at[b, c], kvs, kvr)
     wu_ring = z_ring(lambda b: wu.at[b, x, c], wus, wur)
-    wg_ring = z_ring(lambda b: wg.at[b, :, c], gzs, gzr)
+    wg_rings = [
+        z_ring(lambda b, j=j: wg.at[b, lax.rem(x + j, NX), c], gzs.at[j], gzr.at[j])
+        for j in range(NX)
+    ]
+
+    def wg_step(j, s):
+        ring_step(wg_rings[j], s, lambda k: None)
+        if j == NX - 1:
+            for k in ks(s):
+                wg_hand(k, c).start()
+
 
     def hand_blk(k):
         off = (0, -1, -2, -3, 1, 2, 3, 4)[k]
@@ -188,11 +198,7 @@
         d.wait()
     for i in range(3):
         ow_y(i, y).start()
-    for i in range(3):
-        wg_x(i, x).start()
     ring_start(wu_ring)
-    for i in range(3):
-        wu_x(0, i, x).start()
 
     lane = lax.broadcasted_iota(jnp.int32, (ROWS, 128), 1)
 
@@ -204,11 +210,16 @@
             qz[half, slot, ROWS : 2 * ROWS] = jnp.where(lane < 64, zero, block)
 
     prepare(x)
-    for i in range(3):
+    for i in (1, 2, 0):
         q_copy(i, from_x(i)).wait_recv()
+    for i in range(3):
+        wg_x(i, x).start()
+    for i in range(3):
+        wu_x(0, i, x).start()
+    for i in range(3):
         prepare(from_x(i))
 
-    def piece(pair, slot, masked):
+    def piece(chunk, pair, slot, masked):
         if masked:
             j = lax.broadcasted_iota(jnp.int32, (1, 768), 1)
             second = (j >= 384).astype(jnp.int32)
@@ -226,29 +237,26 @@
             )
             if masked:
                 s = jnp.where(visible, s, HIDE)
-            if masked:
-                new = jnp.broadcast_to(
-                    jnp.maximum(jnp.max(s, axis=1, keepdims=True), FLOOR), (2 * ROWS, 128)
-                )
-            else:
-                old = m[half, slot]
-                new = jnp.maximum(old, jnp.max(s, axis=1, keepdims=True))
-                fade = jnp.exp(old - new)
-            m[half, slot] = new
+            new = jnp.broadcast_to(
+                jnp.maximum(jnp.max(s, axis=1, keepdims=True), FLOOR), (2 * ROWS, 128)
+            )
+            m[chunk, half, slot] = new
             e = jnp.exp(s - new[:, 0:1])
             part_sum = e[:, 0:128]
             for t in range(1, 6):
                 part_sum = part_sum + e[:, t * 128 : (t + 1) * 128]
-            l[half, slot] = part_sum if masked else l[half, slot] * fade + part_sum
+            l[chunk, half, slot] = part_sum
             eb = e.astype(bf16)
             for h in range(2):
                 rows = slice(h * ROWS, (h + 1) * ROWS)
                 vals = kv[pl.ds(2 * pair, 2), :, :, 256 + h * 128 : 384 + h * 128].reshape(768, 128)
-                more = jnp.dot(eb[rows], vals, preferred_element_type=f32)
-                if masked:
-                    acc[half, slot, rows] = more
-                else:
-                    acc[half, slot, rows] = acc[half, slot, rows] * fade[rows] + more
+                acc[chunk, half, slot, rows] = jnp.dot(eb[rows], vals, preferred_element_type=f32)
+
+    def unseen(chunk, slot):
+        for half in range(2):
+            m[chunk, half, slot] = jnp.full((2 * ROWS, 128), FLOOR, f32)
+            l[chunk, half, slot] = jnp.zeros((2 * ROWS, 128), f32)
+            acc[chunk, half, slot] = jnp.zeros((2 * ROWS, 128), f32)
 
     own = z // 2
     odd = z % 2
@@ -259,15 +267,23 @@
         lax.rem(own + 2, 4),
     )
 
-    def sum_stats(slot):
+    def join(slot, take_values):
         st = jnp.zeros((ROWS, 128), f32)
         for half in range(2):
             for h in range(2):
                 rows = slice(h * ROWS, (h + 1) * ROWS)
                 k = half * 2 + h
-                st = jnp.where(lane == k, m[half, slot, rows], st)
-                tot = jnp.sum(l[half, slot, rows], axis=1, keepdims=True)
-                st = jnp.where(lane == 4 + k, tot, st)
+                ms = [m[n, half, slot, rows] for n in range(4)]
+                top = jnp.maximum(jnp.maximum(ms[0], ms[1]), jnp.maximum(ms[2], ms[3]))
+                tot, val = None, None
+                for n in range(4):
+                    w = jnp.exp(ms[n] - top)
+                    t = l[n, half, slot, rows] * w
+                    v = acc[n, half, slot, rows] * w
+                    tot, val = (t, v) if n == 0 else (tot + t, val + v)
+                take_values(half, h, val)
+                st = jnp.where(lane == k, top, st)
+                st = jnp.where(lane == 4 + k, jnp.sum(tot, axis=1, keepdims=True), st)
         return st
 
     def p_copy(i):
@@ -279,73 +295,116 @@
     def i_dx(i):
         return jnp.where(i == 0, 2, jnp.where(i == 1, 1, 3))
 
-    wu_hand_waits = []
-    for ci in range(4):
-        s = ci + 1
+    def wu_spread(k):
+        for i in range(3):
+            wu_x(k, i, x).start()
+
+    def wu_finish(k):
+        for i in range(3):
+            wu_x(k, i, from_x(i)).wait_recv()
+        wu_hand(k, c).start()
+
+    def kv_arrive(s):
         ring_step(kv_ring, s, lambda k: kv_hand(k, c).start())
-        if ci == 0:
-            kv_hand(0, 1 - c).wait_recv()
-        for k in ks(s):
-            kv_hand(k, 1 - c).wait_recv()
-        pair = pairs[ci]
-        if ci == 0:
-            def body0(slot, carry):
-                piece(pair, slot, True)
-                return carry
-            lax.fori_loop(0, 4, body0, 0)
-        elif ci < 3:
-            @pl.when(pair < own)
+
+    def wu_arrive(s, spread):
+        ring_step(wu_ring, s, lambda k: None)
+        for k in spread:
+            wu_spread(k)
+
+    def all_slots(chunk, masked, first):
+        pair = pairs[chunk]
+
+        def body(slot, carry):
+            if masked:
+                piece(chunk, pair, slot, True)
+            else:
+                seen = pair < own
+                pl.when(seen)(lambda: piece(chunk, pair, slot, False))
+                pl.when(jnp.logical_not(seen))(lambda: unseen(chunk, slot))
+            pl.when(slot == 0)(first)
+            return carry
+
+        lax.fori_loop(0, NX, body, 0)
+
+    kv_arrive(1)
+    for k in (0,) + ks(1):
+        kv_hand(k, 1 - c).wait_recv()
+    all_slots(0, True, lambda: wu_arrive(1, ks(1)))
+    for i in range(3):
+        wg_x(i, from_x(i)).wait_recv()
+    wg_hand(0, c).start()
+
+    kv_arrive(2)
+    for k in ks(2):
+        kv_hand(k, 1 - c).wait_recv()
+    all_slots(1, False, lambda: wu_arrive(2, (2,)))
+
+    wu_finish(0)
+    kv_arrive(3)
+    for k in ks(3):
+        kv_hand(k, 1 - c).wait_recv()
+
+    def last(idx, carry):
+        final = jnp.logical_and(idx >= 3, idx != 6)
+        i = jnp.where(idx < 3, idx, jnp.where(idx < 6, idx - 3, 3))
+        slot = lax.rem(x + jnp.where(i == 3, 0, i_dx(i)), NX)
+        chunk = jnp.where(final, 3, 2)
+        pair = jnp.where(final, pairs[3], pairs[2])
+
+        @pl.when(idx == 3)
+        def _():
+            kv_arrive(4)
+            for k in ks(4):
+                kv_hand(k, 1 - c).wait_recv()
+
+        seen = pair < own
+        pl.when(seen)(lambda: piece(chunk, pair, slot, False))
+        pl.when(jnp.logical_not(seen))(lambda: unseen(chunk, slot))
+
+        @pl.when(jnp.logical_and(final, i < 3))
+        def _():
+            def put(half, h, val):
+                col = (half * 2 + h) * 128
+                psend[i, :, col : col + 128] = val.astype(bf16)
+
+            st = jnp.concatenate((join(slot, put), jnp.zeros((64, 128), f32)), axis=0)
+            ssend[i] = st.T[0:8]
+            p_copy(i).start()
+            s_copy(i).start()
+
+        @pl.when(idx == 0)
+        def _():
+            wu_arrive(3, (5,))
+            for ring in wg_rings:
+                ring_start(ring)
+
+        @pl.when(idx == 2)
+        def _():
+            for k in ks(1):
+                wu_finish(k)
+
+        @pl.when(idx == 3)
+        def _():
+            wu_arrive(4, ())
+            wg_step(0, 1)
+
+        for j in (1, 2, 3):
+            @pl.when(idx == 3 + j)
             def _():
-                def body1(slot, carry):
-                    piece(pair, slot, False)
-                    return carry
-                lax.fori_loop(0, 4, body1, 0)
-        else:
-            def body3(i, carry):
-                slot = lax.rem(x + jnp.where(i == 3, 0, i_dx(i)), NX)
-
-                @pl.when(pair < own)
-                def _():
-                    piece(pair, slot, False)
-
-                @pl.when(i < 3)
-                def _():
-                    for half in range(2):
-                        for h in range(2):
-                            col = (half * 2 + h) * 128
-                            psend[i, :, col : col + 128] = acc[
-                                half, slot, h * ROWS : (h + 1) * ROWS
-                            ].astype(bf16)
-                    st = jnp.concatenate((sum_stats(slot), jnp.zeros((64, 128), f32)), axis=0)
-                    ssend[i] = st.T[0:8]
-                    p_copy(i).start()
-                    s_copy(i).start()
-                return carry
-            lax.fori_loop(0, 4, body3, 0)
-
-        ring_step(
-            wu_ring, s,
-            (lambda k: [wu_x(k, i, x).start() for i in range(3)]),
-        )
-        if ci == 0:
-            for i in range(3):
-                wg_x(i, from_x(i)).wait_recv()
-            wg_hand(0, c).start()
-        if ci == 1:
-            for i in range(3):
-                wu_x(0, i, from_x(i)).wait_recv()
-            wu_hand(0, c).start()
-            for k in ks(1):
-                for i in range(3):
-                    wu_x(k, i, from_x(i)).wait_recv()
-                wu_hand(k, c).start()
-        if ci == 2:
-            ring_start(wg_ring)
-            for i in range(3):
-                ow_y(i, from_y(i)).wait_recv()
-                ow_hand(i, c).start()
-
-    ring_step(wg_ring, 1, lambda k: wg_hand(k, c).start())
+                wg_step(j, 1)
+
+        @pl.when(idx == 7)
+        def _():
+            wg_step(0, 2)
+
+        return carry
+
+    lax.fori_loop(0, 8, last, 0)
+    wg_step(1, 2)
+    for i in range(3):
+        ow_y(i, from_y(i)).wait_recv()
+        ow_hand(i, c).start()
 
     def take(i):
         p_copy(i).wait_recv()
@@ -353,7 +412,14 @@
         st = jnp.concatenate((srecv[i], jnp.zeros((120, 256), f32)), axis=0).T[0:ROWS]
         return st
 
-    stats = [sum_stats(x)] + [take(i) for i in range(3)]
+    mine = {}
+
+    def keep(half, h, val):
+        mine[half, h] = val
+
+    stats = [join(x, keep)] + [take(i) for i in range(3)]
+    for k in (3, 6, 7):
+        wu_spread(k)
     for h in range(2):
         parts = []
         for half in range(2):
@@ -364,7 +430,7 @@
             top = functools.reduce(jnp.maximum, ms)
             ws = [jnp.exp(a - top) for a in ms]
             tot = sum(w * t for w, t in zip(ws, ls))
-            joined = acc[half, x, h * ROWS : (h + 1) * ROWS] * ws[0]
+            joined = mine[half, h] * ws[0]
             for i in range(3):
                 joined = joined + precv[i, :, col : col + 128].astype(f32) * ws[i + 1]
             parts.append(joined / tot)
@@ -374,14 +440,11 @@
     for i in range(3):
         heads_y(i, y).start()
 
-    def wu_finish(k):
-        for i in range(3):
-            wu_x(k, i, from_x(i)).wait_recv()
-        wu_hand(k, c).start()
-
-    for k in ks(2):
-        wu_finish(k)
-    ring_step(wg_ring, 2, lambda k: wg_hand(k, c).start())
+    wg_step(2, 2)
+    wu_finish(2)
+    wg_step(3, 2)
+    wg_step(0, 3)
+    wg_step(1, 3)
 
     loads[8].wait()
     loads[9].wait()
@@ -397,31 +460,48 @@
             total = total + jnp.dot(heads[yy], ow[yy, :, cols], preferred_element_type=f32)
         stream[:, :, cols] = total.reshape(NY, ROWS // NY, 512)
     rows = stream[...].reshape(ROWS, width)
-    ffn[...] = rms_scale(rows, mix_gain[...]).astype(bf16)
-
-    for k in ks(3):
-        wu_finish(k)
-    ring_step(wg_ring, 3, lambda k: wg_hand(k, c).start())
-    wu_finish(7)
-    ring_step(wg_ring, 4, lambda k: wg_hand(k, c).start())
-    for k in range(8):
+    normed = rms_scale(rows, mix_gain[...]).astype(bf16)
+    for zz in range(NZ):
+        ffn[zz] = normed[:, zz * 256 : (zz + 1) * 256]
+
+    ff = hidden.shape[1]
+    order = (0,) + ks(1) + ks(2) + ks(3) + ks(4)
+    for n, k in enumerate(order):
+        if n == 0:
+            wu_finish(5)
+            wg_step(2, 3)
+        if n == 1:
+            wg_step(3, 3)
+        if n == 2:
+            wu_finish(3)
+            wg_step(0, 4)
+        if n == 3:
+            wg_step(1, 4)
+        if n == 4:
+            wu_finish(6)
+            wg_step(2, 4)
+        if n == 5:
+            wg_step(3, 4)
+            wu_finish(7)
+        wg_hand(k, 1 - c).wait_recv()
         wu_hand(k, 1 - c).wait_recv()
-    ff = hidden.shape[1]
-    for n in range(0, ff, 256):
-        cols = slice(n, min(n + 256, ff))
-        w = wu[:, :, :, :, cols].reshape(width, -1)
-        pre = jnp.dot(ffn[...], w, preferred_element_type=f32).astype(bf16).astype(f32)
-        up_pad[8 : 8 + ROWS, cols] = pre
-    for k in range(8):
-        wg_hand(k, 1 - c).wait_recv()
-    for n in range(0, ff, 256):
-        cols = slice(n, min(n + 256, ff))
-        w = wg[:, :, :, :, cols].reshape(width, -1)
-        pre = jnp.dot(ffn[...], w, preferred_element_type=f32).astype(bf16).astype(f32)
-        gate_pad[8 : 8 + ROWS, cols] = pre
-    edge_out[0] = gate_pad[6 + ROWS : 8 + ROWS, :]
-    edge_out[1] = up_pad[6 + ROWS : 8 + ROWS, :]
-    edge_copy().start()
+        blk = hand_blk(k)
+        rows_in = ffn[blk]
+        if n == 7:
+            for e, (w, pad) in enumerate(((wg, gate_pad), (wu, up_pad))):
+                tip = jnp.dot(
+                    rows_in[ROWS - 16 :], w[blk].reshape(256, ff), preferred_element_type=f32
+                )
+                tip = (tip[8:] + pad[ROWS : 8 + ROWS, :]).astype(bf16).astype(f32)
+                edge_out[e] = tip[6:8]
+            edge_copy().start()
+        for w, pad in ((wg, gate_pad), (wu, up_pad)):
+            pre = jnp.dot(rows_in, w[blk].reshape(256, ff), preferred_element_type=f32)
+            if n > 0:
+                pre = pre + pad[8 : 8 + ROWS, :]
+            if n == 7:
+                pre = pre.astype(bf16).astype(f32)
+            pad[8 : 8 + ROWS, :] = pre
 
     def mix(top, size):
         for n in range(0, ff, 128):
@@ -446,14 +526,6 @@
         part[n] = down.astype(bf16).reshape(NY, ROWS // NY, 512)
         for i in range(3):
             down_y(i, n).start()
-    for n in range(NY):
-        cols = slice(n * 512, (n + 1) * 512)
-        total = stream[y, :, cols] + part[n, y].astype(f32)
-        for i in range(3):
-            down_y(i, n).wait_recv()
-            total = total + drecv[i, n].astype(f32)
-        out[:, cols] = total.astype(bf16)
-
     edge_copy().wait_send()
     for i in range(3):
         q_copy(i, x).wait_send()
@@ -463,9 +535,7 @@
         ow_y(i, y).wait_send()
         ow_hand(i, c).wait_send()
         heads_y(i, y).wait_send()
-        for n in range(NY):
-            down_y(i, n).wait_send()
-    for ring in (kv_ring, wu_ring, wg_ring):
+    for ring in [kv_ring, wu_ring] + wg_rings:
         for s in range(1, 5):
             only(plus_n, s, lambda: ring[0](s).wait_send())
             only(minus_n, s, lambda: ring[1](s).wait_send())
@@ -475,6 +545,16 @@
         wu_hand(k, c).wait_send()
         for i in range(3):
             wu_x(k, i, x).wait_send()
+    for n in range(NY):
+        cols = slice(n * 512, (n + 1) * 512)
+        total = stream[y, :, cols] + part[n, y].astype(f32)
+        for i in range(3):
+            down_y(i, n).wait_recv()
+            total = total + drecv[i, n].astype(f32)
+        out[:, cols] = total.astype(bf16)
+    for i in range(3):
+        for n in range(NY):
+            down_y(i, n).wait_send()
 
 
 def layer(*args):
@@ -484,7 +564,7 @@
     ff, width = args[5].shape[1], args[8].shape[1]
     dma = pltpu.SemaphoreType.DMA
     sems = [(10,), (2, 3), (2, 4), (2, 4), (8,), (8,), (2, 4), (2, 4), (8, 3), (8, 3), (8,), (8,)]
-    sems += [(3,), (3,), (2, 4), (2, 4), (8,), (8,), (3,), (3,), (3,), (3,)]
+    sems += [(3,), (3,), (NX, 2, 4), (NX, 2, 4), (8,), (8,), (3,), (3,), (3,), (3,)]
     sems += [(3,), (3,), (3,), (3,), (3,), (3,), None, None, (3, 4), (3, 4)]
     return pl.pallas_call(
         layer_kernel,
@@ -497,9 +577,9 @@
             pltpu.VMEM((8, 4, 2, 32, ff), bf16),
             pltpu.VMEM((8, 4, 2, 32, ff), bf16),
             pltpu.VMEM((2, 4, 2 * ROWS, 128), bf16),
-            pltpu.VMEM((2, 4, 2 * ROWS, 128), f32),
-            pltpu.VMEM((2, 4, 2 * ROWS, 128), f32),
-            pltpu.VMEM((2, 4, 2 * ROWS, 128), f32),
+            pltpu.VMEM((4, 2, 4, 2 * ROWS, 128), f32),
+            pltpu.VMEM((4, 2, 4, 2 * ROWS, 128), f32),
+            pltpu.VMEM((4, 2, 4, 2 * ROWS, 128), f32),
             pltpu.VMEM((3, ROWS, 512), bf16),
             pltpu.VMEM((3, ROWS, 512), bf16),
             pltpu.VMEM((3, 8, 256), f32),
@@ -509,7 +589,7 @@
             pltpu.VMEM((ff, width), bf16),
             pltpu.VMEM((ROWS, width), bf16),
             pltpu.VMEM((NY, ROWS // NY, width), f32),
-            pltpu.VMEM((ROWS, width), bf16),
+            pltpu.VMEM((NZ, ROWS, 256), bf16),
             pltpu.VMEM((8 + ROWS, ff), f32),
             pltpu.VMEM((8 + ROWS, ff), f32),
             pltpu.VMEM((ROWS, ff), bf16),

time: 97.9 us -> 84.5 us (0.86)
  Pallas kernels: 95.8 us -> 82.7 us
    pallas_call x1, Pallas kernels: 95.8 us -> 82.7 us  [layer(): pl.pallas_call(layer_kernel, out_shape=jax.ShapeDtypeStruct((ROWS // NY,...]
where the time goes in v3:
time: 84.5 us; the launch traced here: 84.3 us
  Pallas kernels  82.7 us (98%)
  local copies, waits for them, and re-layouts  1.62 us (2%)
    pallas_call x1, Pallas kernels, layer(): pl.pallas_call(layer_kernel, out_shape=jax.ShapeDtypeStruct((ROWS // NY,...  82.7 us

profile of v3, /device:TPU:8, one launch (start us, length us, event | category | flops | bytes accessed | tf_op | source)
XLA Modules:
  0.0 84.3 jit_solution(3901266999777276276)
XLA Ops:
  0.0 82.7 %layer.1 = bf16[48,2048]{1,0:T(8,128)(2,1)} custom-call(bf16[192,128]{1,0:T(8,128)(2,1)} %qa.1, bf16[192,128]{1,0:T(8,128)(2,1)} %qb.1, bf16[192,128]{1,0:T(8,128)(2,1)} %ka.1, bf16[192,128]{1,0:T(8,128)(2,1)} %kb.1, bf16[192,256]{1,0:T(8,128)(2,1)} %va.1, bf16[32,1408]{1,0:T(8,128)(2,1)} %gw.1, bf16[32,1408]{1,0:T(8,128)(2,1)} %uw.1, ...), custom_call_target="tpu_custom_call" | custom-call | tf_op jit(solution)/shard_map/layer/pallas_call | solution.py:569
  82.7 1.6 %copy.17 = bf16[48,2048]{1,0:T(8,128)(2,1)} copy(bf16[48,2048]{1,0:T(8,128)(2,1)} %layer.1) | data formatting | bytes 393216

commit v4 on v3

--- a/solution.py
+++ b/solution.py
@@ -25,9 +25,8 @@
     qa, qb, ka, kb, va, gw, uw, out_w, res_in, down_w, lam, gain, mix_gain, gate_taps, up_taps,
     out,
     q, kv, wg, wu, qz, m, l, acc, psend, precv, ssend, srecv,
-    heads, ow, dw, res, stream, ffn, gate_pad, up_pad, hidden, edge_out, edge_in, part, drecv,
-    loc, bar_q, kvs, kvr, kds, kdr, wus, wur, wxs, wxr, wds, wdr, gxs, gxr, gzs, gzr, gds, gdr, pts, ptr, sts, str_,
-    hys, hyr, oys, oyr, ods, odr, es, er, dys, dyr,
+    heads, ow, dw, res, stream, ffn, pad, hidden, edge_out, edge_in, part, drecv,
+    loc, snd, one, hsr, kvr, kdr, wur, wxr, wdr, gzr, gdr, dyr,
 ):
     r = lax.axis_index("sp")
     y = lax.axis_index("tp")
@@ -44,14 +43,16 @@
             src_ref=src, dst_ref=dst, send_sem=ss, recv_sem=rs, device_id=dev, device_id_type=MESH
         )
 
+    cut, ff = wg.shape[4], hidden.shape[1]
     loads = [
         (qa, q.at[x, :, 0:128]),
         (qb, q.at[x, :, 128:256]),
         (ka, kv.at[z, c, :, 0:128]),
         (kb, kv.at[z, c, :, 128:256]),
         (va, kv.at[z, c, :, 256:512]),
-        (gw, wg.at[z, x, c]),
-        (uw, wu.at[z, x, c]),
+        (gw.at[:, 0:cut], wg.at[z, x, c]),
+        (gw.at[:, cut:ff], wu.at[z, x, c, :, 0 : ff - cut]),
+        (uw, wu.at[z, x, c, :, ff - cut : 2 * ff - cut]),
         (out_w, ow.at[y]),
         (res_in, res),
         (down_w, dw),
@@ -70,26 +71,26 @@
         d.wait()
 
     def q_copy(i, slot):
-        return rcopy(q.at[slot], q.at[slot], bar_q.at[0, i], bar_q.at[1, i], at(z, x + DX[i], c))
+        return rcopy(q.at[slot], q.at[slot], snd.at[0], one.at[0], at(z, x + DX[i], c))
 
     plus_n, minus_n = 4 - c, 3 + c
 
     def z_ring(ref_at, sends, recvs):
         def plus(s):
             blk = lax.rem(z - s + 1 + NZ, NZ)
-            return rcopy(ref_at(blk), ref_at(blk), sends.at[0, s - 1], recvs.at[0, s - 1], up_dev)
+            return rcopy(ref_at(blk), ref_at(blk), sends, recvs.at[0, s - 1], up_dev)
 
         def minus(s):
             blk = lax.rem(z + s - 1, NZ)
-            return rcopy(ref_at(blk), ref_at(blk), sends.at[1, s - 1], recvs.at[1, s - 1], down_dev)
+            return rcopy(ref_at(blk), ref_at(blk), sends, recvs.at[1, s - 1], down_dev)
 
         def plus_in(s):
             blk = lax.rem(z - s + NZ, NZ)
-            return rcopy(ref_at(blk), ref_at(blk), sends.at[0, s - 1], recvs.at[0, s - 1], up_dev)
+            return rcopy(ref_at(blk), ref_at(blk), sends, recvs.at[0, s - 1], up_dev)
 
         def minus_in(s):
             blk = lax.rem(z + s, NZ)
-            return rcopy(ref_at(blk), ref_at(blk), sends.at[1, s - 1], recvs.at[1, s - 1], down_dev)
+            return rcopy(ref_at(blk), ref_at(blk), sends, recvs.at[1, s - 1], down_dev)
 
         return plus, minus, plus_in, minus_in
 
@@ -99,10 +100,13 @@
         elif s == 4:
             pl.when(n == 4)(fn)
 
-    kv_ring = z_ring(lambda b: kv.at[b, c], kvs, kvr)
-    wu_ring = z_ring(lambda b: wu.at[b, x, c], wus, wur)
+    kv_rings = [
+        z_ring(lambda b, h=h: kv.at[b, c, h * 96 : (h + 1) * 96], snd.at[1], kvr.at[h])
+        for h in range(2)
+    ]
+    wu_ring = z_ring(lambda b: wu.at[b, x, c], snd.at[2], wur)
     wg_rings = [
-        z_ring(lambda b, j=j: wg.at[b, lax.rem(x + j, NX), c], gzs.at[j], gzr.at[j])
+        z_ring(lambda b, j=j: wg.at[b, lax.rem(x + j, NX), c], snd.at[3], gzr.at[j])
         for j in range(NX)
     ]
 
@@ -119,22 +123,34 @@
 
     def kv_hand(k, lane):
         b = hand_blk(k)
-        return rcopy(kv.at[b, lane], kv.at[b, lane], kds.at[k], kdr.at[k], mate)
+        return rcopy(kv.at[b, lane], kv.at[b, lane], snd.at[4], kdr.at[k], mate)
 
     def wg_hand(k, lane):
         b = hand_blk(k)
-        return rcopy(wg.at[b, :, lane], wg.at[b, :, lane], gds.at[k], gdr.at[k], mate)
+        return rcopy(wg.at[b, :, lane], wg.at[b, :, lane], snd.at[5], gdr.at[k], mate)
 
     def wu_hand(k, lane):
         b = hand_blk(k)
-        return rcopy(wu.at[b, :, lane], wu.at[b, :, lane], wds.at[k], wdr.at[k], mate)
-
-    def wu_x(k, i, xx):
-        b = hand_blk(k)
-        return rcopy(wu.at[b, xx, c], wu.at[b, xx, c], wxs.at[k, i], wxr.at[k, i], at(z, x + DX[i], c))
+        return rcopy(wu.at[b, :, lane], wu.at[b, :, lane], snd.at[6], wdr.at[k], mate)
+
+    toward = 1 - 2 * c
+
+    def wu_x(k, d):
+        ref = wu.at[hand_blk(k), x, c]
+        return rcopy(ref, ref, snd.at[7], wxr.at[k, 0], at(z, x + d, c))
+
+    def wu_x2(k):
+        ref = wu.at[hand_blk(k), lax.rem(x - toward + NX, NX), c]
+        return rcopy(ref, ref, snd.at[8], wxr.at[k, 1], at(z, x + toward, c))
 
     def wg_x(i, xx):
-        return rcopy(wg.at[z, xx, c], wg.at[z, xx, c], gxs.at[i], gxr.at[i], at(z, x + DX[i], c))
+        return rcopy(wg.at[z, xx, c], wg.at[z, xx, c], snd.at[9], one.at[1], at(z, x + DX[i], c))
+
+    def got(ref, sem):
+        rcopy(ref, ref, snd.at[0], sem, mate).wait_recv()
+
+    def gone(ref, n):
+        rcopy(ref, ref, snd.at[n], one.at[0], mate).wait_send()
 
     def from_x(i):
         return lax.rem(x - DX[i] + NX, NX)
@@ -173,28 +189,29 @@
 
     def ow_y(i, yy):
         ref = ow.at[yy, :, pl.ds(pl.multiple_of(c * half_cols, 128), half_cols)]
-        return rcopy(ref, ref, oys.at[i], oyr.at[i], across[i])
+        return rcopy(ref, ref, snd.at[10], one.at[2], across[i])
 
     def ow_hand(i, lane):
         ref = ow.at[from_y(i), :, pl.ds(pl.multiple_of(lane * half_cols, 128), half_cols)]
-        return rcopy(ref, ref, ods.at[i], odr.at[i], mate)
+        return rcopy(ref, ref, snd.at[11], one.at[3], mate)
 
     def heads_y(i, yy):
-        return rcopy(heads.at[yy], heads.at[yy], hys.at[i], hyr.at[i], across[i])
+        return rcopy(heads.at[yy], heads.at[yy], snd.at[12], hsr.at[i], across[i])
 
     def edge_copy():
-        return rcopy(edge_out, edge_in, es, er, after)
+        return rcopy(edge_out, edge_in, snd.at[13], one.at[5], after)
 
     def down_y(i, n):
         return rcopy(
-            part.at[n, across[i][1]], drecv.at[i, n], dys.at[i, n], dyr.at[i, n], across[i]
+            part.at[n, across[i][1]], drecv.at[i, n], snd.at[14], dyr.at[n], across[i]
         )
 
     for i in range(3):
         q_copy(i, x).start()
-    ring_start(kv_ring)
+    ring_start(kv_rings[0])
+    ring_start(kv_rings[1])
     kv_hand(0, c).start()
-    for d in loads[5:8]:
+    for d in loads[5:9]:
         d.wait()
     for i in range(3):
         ow_y(i, y).start()
@@ -210,12 +227,13 @@
             qz[half, slot, ROWS : 2 * ROWS] = jnp.where(lane < 64, zero, block)
 
     prepare(x)
-    for i in (1, 2, 0):
-        q_copy(i, from_x(i)).wait_recv()
+    ring_step(kv_rings[0], 1, lambda k: None)
     for i in range(3):
         wg_x(i, x).start()
-    for i in range(3):
-        wu_x(0, i, x).start()
+    wu_x(0, 1).start()
+    wu_x(0, 3).start()
+    ring_step(kv_rings[1], 1, lambda k: kv_hand(k, c).start())
+    got(q.at[0:3], one.at[0])
     for i in range(3):
         prepare(from_x(i))
 
@@ -287,32 +305,35 @@
         return st
 
     def p_copy(i):
-        return rcopy(psend.at[i], precv.at[i], pts.at[i], ptr.at[i], (at(z, x + i_dx(i), c)))
+        return rcopy(psend.at[i], precv.at[i], snd.at[15], one.at[6], (at(z, x + i_dx(i), c)))
 
     def s_copy(i):
-        return rcopy(ssend.at[i], srecv.at[i], sts.at[i], str_.at[i], (at(z, x + i_dx(i), c)))
+        return rcopy(ssend.at[i], srecv.at[i], snd.at[16], one.at[7], (at(z, x + i_dx(i), c)))
 
     def i_dx(i):
         return jnp.where(i == 0, 2, jnp.where(i == 1, 1, 3))
 
     def wu_spread(k):
-        for i in range(3):
-            wu_x(k, i, x).start()
+        wu_x(k, 1).start()
+        wu_x(k, 3).start()
+
+    def wu_mid(k):
+        got(wu.at[0, 0:2, c], wxr.at[k, 0])
+        wu_x2(k).start()
 
     def wu_finish(k):
-        for i in range(3):
-            wu_x(k, i, from_x(i)).wait_recv()
+        got(wu.at[0, 0, c], wxr.at[k, 1])
         wu_hand(k, c).start()
 
-    def kv_arrive(s):
-        ring_step(kv_ring, s, lambda k: kv_hand(k, c).start())
+    def kv_arrive(s, h):
+        ring_step(kv_rings[h], s, lambda k: kv_hand(k, c).start() if h == 1 else None)
 
     def wu_arrive(s, spread):
         ring_step(wu_ring, s, lambda k: None)
         for k in spread:
             wu_spread(k)
 
-    def all_slots(chunk, masked, first):
+    def all_slots(chunk, masked, first, s):
         pair = pairs[chunk]
 
         def body(slot, carry):
@@ -323,25 +344,21 @@
                 pl.when(seen)(lambda: piece(chunk, pair, slot, False))
                 pl.when(jnp.logical_not(seen))(lambda: unseen(chunk, slot))
             pl.when(slot == 0)(first)
+            pl.when(slot == 1)(lambda: kv_arrive(s, 0))
+            pl.when(slot == (3 if masked else 2))(lambda: kv_arrive(s, 1))
             return carry
 
         lax.fori_loop(0, NX, body, 0)
 
-    kv_arrive(1)
     for k in (0,) + ks(1):
         kv_hand(k, 1 - c).wait_recv()
-    all_slots(0, True, lambda: wu_arrive(1, ks(1)))
-    for i in range(3):
-        wg_x(i, from_x(i)).wait_recv()
+    all_slots(0, True, lambda: wu_arrive(1, ks(1)), 2)
+    got(wg.at[0, 0:3, c], one.at[1])
     wg_hand(0, c).start()
-
-    kv_arrive(2)
+    wu_mid(0)
     for k in ks(2):
         kv_hand(k, 1 - c).wait_recv()
-    all_slots(1, False, lambda: wu_arrive(2, (2,)))
-
-    wu_finish(0)
-    kv_arrive(3)
+    all_slots(1, False, lambda: wu_arrive(2, ks(2)), 3)
     for k in ks(3):
         kv_hand(k, 1 - c).wait_recv()
 
@@ -354,7 +371,6 @@
 
         @pl.when(idx == 3)
         def _():
-            kv_arrive(4)
             for k in ks(4):
                 kv_hand(k, 1 - c).wait_recv()
 
@@ -375,14 +391,20 @@
 
         @pl.when(idx == 0)
         def _():
-            wu_arrive(3, (5,))
+            wu_arrive(3, ())
             for ring in wg_rings:
                 ring_start(ring)
 
+        @pl.when(idx == 1)
+        def _():
+            wu_finish(0)
+            for k in ks(1):
+                wu_mid(k)
+
         @pl.when(idx == 2)
         def _():
-            for k in ks(1):
-                wu_finish(k)
+            kv_arrive(4, 0)
+            kv_arrive(4, 1)
 
         @pl.when(idx == 3)
         def _():
@@ -394,21 +416,30 @@
             def _():
                 wg_step(j, 1)
 
+        @pl.when(idx == 5)
+        def _():
+            for k in ks(1):
+                wu_finish(k)
+
         @pl.when(idx == 7)
         def _():
             wg_step(0, 2)
+            for k in ks(2):
+                wu_mid(k)
 
         return carry
 
     lax.fori_loop(0, 8, last, 0)
+    for k in (3, 6, 7):
+        wu_spread(k)
     wg_step(1, 2)
+    wg_step(2, 2)
+    wg_step(3, 2)
+    got(ow.at[0:3, :, 0:half_cols], one.at[2])
     for i in range(3):
-        ow_y(i, from_y(i)).wait_recv()
         ow_hand(i, c).start()
 
     def take(i):
-        p_copy(i).wait_recv()
-        s_copy(i).wait_recv()
         st = jnp.concatenate((srecv[i], jnp.zeros((120, 256), f32)), axis=0).T[0:ROWS]
         return st
 
@@ -417,9 +448,10 @@
     def keep(half, h, val):
         mine[half, h] = val
 
-    stats = [join(x, keep)] + [take(i) for i in range(3)]
-    for k in (3, 6, 7):
-        wu_spread(k)
+    stats = [join(x, keep)]
+    got(precv, one.at[6])
+    got(srecv, one.at[7])
+    stats += [take(i) for i in range(3)]
     for h in range(2):
         parts = []
         for half in range(2):
@@ -440,84 +472,93 @@
     for i in range(3):
         heads_y(i, y).start()
 
-    wg_step(2, 2)
-    wu_finish(2)
-    wg_step(3, 2)
     wg_step(0, 3)
+    for k in ks(2):
+        wu_finish(k)
     wg_step(1, 3)
-
-    loads[8].wait()
+    wu_mid(3)
+    wg_step(2, 3)
+    wg_step(3, 3)
+    wu_mid(6)
+
     loads[9].wait()
-    for i in range(3):
-        ow_hand(i, 1 - c).wait_recv()
-    for i in range(3):
-        heads_y(i, from_y(i)).wait_recv()
+    loads[10].wait()
+    got(ow.at[0:3, :, 0:half_cols], one.at[3])
     width = stream.shape[2]
-    for n in range(0, width, 512):
-        cols = slice(n, n + 512)
-        total = res[:, cols].astype(f32)
-        for yy in range(NY):
-            total = total + jnp.dot(heads[yy], ow[yy, :, cols], preferred_element_type=f32)
-        stream[:, :, cols] = total.reshape(NY, ROWS // NY, 512)
+    for i in (None, 1, 2, 0):
+        yy = y
+        if i is not None:
+            yy = from_y(i)
+            heads_y(i, yy).wait_recv()
+        for n in range(0, width, 512):
+            cols = slice(n, n + 512)
+            more = jnp.dot(heads[yy], ow[yy, :, cols], preferred_element_type=f32)
+            more = more.reshape(NY, ROWS // NY, 512)
+            if i is None:
+                more = more + res[:, cols].astype(f32).reshape(NY, ROWS // NY, 512)
+            else:
+                more = more + stream[:, :, cols]
+            stream[:, :, cols] = more
     rows = stream[...].reshape(ROWS, width)
     normed = rms_scale(rows, mix_gain[...]).astype(bf16)
     for zz in range(NZ):
         ffn[zz] = normed[:, zz * 256 : (zz + 1) * 256]
 
-    ff = hidden.shape[1]
     order = (0,) + ks(1) + ks(2) + ks(3) + ks(4)
-    for n, k in enumerate(order):
+    pieces = ((wg, slice(0, cut)), (wu, slice(cut, 2 * ff)))
+    for n in range(0, 8, 2):
+        two = order[n : n + 2]
         if n == 0:
-            wu_finish(5)
-            wg_step(2, 3)
-        if n == 1:
-            wg_step(3, 3)
+            wg_step(0, 4)
+            wu_mid(7)
         if n == 2:
+            wg_step(1, 4)
+            wg_step(2, 4)
             wu_finish(3)
-            wg_step(0, 4)
-        if n == 3:
-            wg_step(1, 4)
         if n == 4:
             wu_finish(6)
-            wg_step(2, 4)
-        if n == 5:
             wg_step(3, 4)
             wu_finish(7)
-        wg_hand(k, 1 - c).wait_recv()
-        wu_hand(k, 1 - c).wait_recv()
-        blk = hand_blk(k)
-        rows_in = ffn[blk]
-        if n == 7:
-            for e, (w, pad) in enumerate(((wg, gate_pad), (wu, up_pad))):
-                tip = jnp.dot(
-                    rows_in[ROWS - 16 :], w[blk].reshape(256, ff), preferred_element_type=f32
-                )
-                tip = (tip[8:] + pad[ROWS : 8 + ROWS, :]).astype(bf16).astype(f32)
-                edge_out[e] = tip[6:8]
+        for k in two:
+            wg_hand(k, 1 - c).wait_recv()
+            wu_hand(k, 1 - c).wait_recv()
+        blks = [hand_blk(k) for k in two]
+
+        def product(w, top):
+            return sum(
+                jnp.dot(ffn[b, top:], w[b].reshape(256, -1), preferred_element_type=f32)
+                for b in blks
+            )
+
+        if n == 6:
+            for w, cols in pieces:
+                tip = product(w, ROWS - 16)
+                tip = (tip[8:] + pad[ROWS : 8 + ROWS, cols]).astype(bf16).astype(f32)
+                edge_out[:, cols] = tip[6:8]
             edge_copy().start()
-        for w, pad in ((wg, gate_pad), (wu, up_pad)):
-            pre = jnp.dot(rows_in, w[blk].reshape(256, ff), preferred_element_type=f32)
+        for w, cols in pieces:
+            pre = product(w, 0)
             if n > 0:
-                pre = pre + pad[8 : 8 + ROWS, :]
-            if n == 7:
+                pre = pre + pad[8 : 8 + ROWS, cols]
+            if n == 6:
                 pre = pre.astype(bf16).astype(f32)
-            pad[8 : 8 + ROWS, :] = pre
+            pad[8 : 8 + ROWS, cols] = pre
 
     def mix(top, size):
         for n in range(0, ff, 128):
             cols = slice(n, n + 128)
             conv = []
-            for pad, taps in ((gate_pad, gate_taps), (up_pad, up_taps)):
-                v = taps[0:1, cols] * pad[6 + top : 6 + top + size, cols]
-                v = v + taps[1:2, cols] * pad[7 + top : 7 + top + size, cols]
-                v = v + taps[2:3, cols] * pad[8 + top : 8 + top + size, cols]
+            for base, taps in ((0, gate_taps), (ff, up_taps)):
+                there = slice(base + n, base + n + 128)
+                v = taps[0:1, cols] * pad[6 + top : 6 + top + size, there]
+                v = v + taps[1:2, cols] * pad[7 + top : 7 + top + size, there]
+                v = v + taps[2:3, cols] * pad[8 + top : 8 + top + size, there]
                 conv.append(v)
             hidden[top : top + size, cols] = (jax.nn.silu(conv[0]) * conv[1]).astype(bf16)
 
     mix(16, ROWS - 16)
     edge_copy().wait_recv()
-    gate_pad[6:8, :] = jnp.where(r == 0, 0.0, edge_in[0])
-    up_pad[6:8, :] = jnp.where(r == 0, 0.0, edge_in[1])
+    pad[6:8, :] = jnp.where(r == 0, 0.0, edge_in[...])
     mix(0, 16)
 
     for n in range(NY):
@@ -527,34 +568,29 @@
         for i in range(3):
             down_y(i, n).start()
     edge_copy().wait_send()
-    for i in range(3):
-        q_copy(i, x).wait_send()
-        wg_x(i, x).wait_send()
-        p_copy(i).wait_send()
-        s_copy(i).wait_send()
-        ow_y(i, y).wait_send()
-        ow_hand(i, c).wait_send()
-        heads_y(i, y).wait_send()
-    for ring in [kv_ring, wu_ring] + wg_rings:
-        for s in range(1, 5):
-            only(plus_n, s, lambda: ring[0](s).wait_send())
-            only(minus_n, s, lambda: ring[1](s).wait_send())
-    for k in range(8):
-        kv_hand(k, c).wait_send()
-        wg_hand(k, c).wait_send()
-        wu_hand(k, c).wait_send()
-        for i in range(3):
-            wu_x(k, i, x).wait_send()
+    gone(q.at[0:3], 0)
+    gone(kv.at[0:7, 0], 1)
+    gone(wu.at[0:7, 0, 0], 2)
+    gone(wg.at[0:7, :, 0], 3)
+    gone(kv.at[:, 0], 4)
+    gone(wg.at[:, :, 0], 5)
+    gone(wu.at[:, :, 0], 6)
+    gone(wu.at[:, 0:2, 0], 7)
+    gone(wu.at[:, 0, 0], 8)
+    gone(wg.at[0, 0:3, 0], 9)
+    gone(ow.at[0:3, :, 0:half_cols], 10)
+    gone(ow.at[0:3, :, 0:half_cols], 11)
+    gone(heads.at[0:3], 12)
+    gone(psend, 15)
+    gone(ssend, 16)
     for n in range(NY):
         cols = slice(n * 512, (n + 1) * 512)
         total = stream[y, :, cols] + part[n, y].astype(f32)
+        got(drecv.at[:, n], dyr.at[n])
         for i in range(3):
-            down_y(i, n).wait_recv()
             total = total + drecv[i, n].astype(f32)
         out[:, cols] = total.astype(bf16)
-    for i in range(3):
-        for n in range(NY):
-            down_y(i, n).wait_send()
+    gone(drecv, 14)
 
 
 def layer(*args):
@@ -563,9 +599,8 @@
     SM = pl.BlockSpec(memory_space=pltpu.SMEM)
     ff, width = args[5].shape[1], args[8].shape[1]
     dma = pltpu.SemaphoreType.DMA
-    sems = [(10,), (2, 3), (2, 4), (2, 4), (8,), (8,), (2, 4), (2, 4), (8, 3), (8, 3), (8,), (8,)]
-    sems += [(3,), (3,), (NX, 2, 4), (NX, 2, 4), (8,), (8,), (3,), (3,), (3,), (3,)]
-    sems += [(3,), (3,), (3,), (3,), (3,), (3,), None, None, (3, 4), (3, 4)]
+    cut = 9 * 128 if ff > 9 * 128 else ff // 2
+    sems = [(11,), (17,), (8,), (3,), (2, 2, 4), (8,), (2, 4), (8, 2), (8,), (NX, 2, 4), (8,), (NY,)]
     return pl.pallas_call(
         layer_kernel,
         out_shape=jax.ShapeDtypeStruct((ROWS // NY, width), bf16),
@@ -574,8 +609,8 @@
         scratch_shapes=[
             pltpu.VMEM((4, ROWS, 256), bf16),
             pltpu.VMEM((8, 2, ROWS, 512), bf16),
-            pltpu.VMEM((8, 4, 2, 32, ff), bf16),
-            pltpu.VMEM((8, 4, 2, 32, ff), bf16),
+            pltpu.VMEM((8, 4, 2, 32, cut), bf16),
+            pltpu.VMEM((8, 4, 2, 32, 2 * ff - cut), bf16),
             pltpu.VMEM((2, 4, 2 * ROWS, 128), bf16),
             pltpu.VMEM((4, 2, 4, 2 * ROWS, 128), f32),
             pltpu.VMEM((4, 2, 4, 2 * ROWS, 128), f32),
@@ -590,14 +625,13 @@
             pltpu.VMEM((ROWS, width), bf16),
             pltpu.VMEM((NY, ROWS // NY, width), f32),
             pltpu.VMEM((NZ, ROWS, 256), bf16),
-            pltpu.VMEM((8 + ROWS, ff), f32),
-            pltpu.VMEM((8 + ROWS, ff), f32),
+            pltpu.VMEM((8 + ROWS, 2 * ff), f32),
             pltpu.VMEM((ROWS, ff), bf16),
-            pltpu.VMEM((2, 2, ff), f32),
-            pltpu.VMEM((2, 2, ff), f32),
+            pltpu.VMEM((2, 2 * ff), f32),
+            pltpu.VMEM((2, 2 * ff), f32),
             pltpu.VMEM((NY, NY, ROWS // NY, 512), bf16),
             pltpu.VMEM((3, NY, ROWS // NY, 512), bf16),
-        ] + [dma if s is None else dma(s) for s in sems],
+        ] + [dma(s) for s in sems],
         compiler_params=pltpu.CompilerParams(
             collective_id=0, has_side_effects=True, vmem_limit_bytes=63 * 1024 * 1024
         ),

time: 84.5 us -> 79.8 us (0.944)
  Pallas kernels: 82.7 us -> 78 us
    pallas_call x1, Pallas kernels: 82.7 us -> 78 us  [layer(): pl.pallas_call(layer_kernel, out_shape=jax.ShapeDtypeStruct((ROWS // NY,...]
where the time goes in v4:
time: 79.8 us; the launch traced here: 79.6 us
  Pallas kernels  78 us (98%)
  local copies, waits for them, and re-layouts  1.62 us (2%)
    pallas_call x1, Pallas kernels, layer(): pl.pallas_call(layer_kernel, out_shape=jax.ShapeDtypeStruct((ROWS // NY,...  78 us
    unnamed x1, local copies, waits for them, and re-layouts  1.62 us

profile of v4, /device:TPU:8, one launch (start us, length us, event | category | flops | bytes accessed | tf_op | source)
XLA Modules:
  0.0 79.6 jit_solution(10596413875880252590)
XLA Ops:
  0.0 78.0 %layer.1 = bf16[48,2048]{1,0:T(8,128)(2,1)} custom-call(bf16[192,128]{1,0:T(8,128)(2,1)} %qa.1, bf16[192,128]{1,0:T(8,128)(2,1)} %qb.1, bf16[192,128]{1,0:T(8,128)(2,1)} %ka.1, bf16[192,128]{1,0:T(8,128)(2,1)} %kb.1, bf16[192,256]{1,0:T(8,128)(2,1)} %va.1, bf16[32,1408]{1,0:T(8,128)(2,1)} %gw.1, bf16[32,1408]{1,0:T(8,128)(2,1)} %uw.1, ...), custom_call_target="tpu_custom_call" | custom-call | tf_op jit(solution)/shard_map/layer/pallas_call | solution.py:604
  78.0 1.6 %copy.17 = bf16[48,2048]{1,0:T(8,128)(2,1)} copy(bf16[48,2048]{1,0:T(8,128)(2,1)} %layer.1) | data formatting | bytes 393216

commit v5 on v4

--- a/solution.py
+++ b/solution.py
@@ -405,6 +405,8 @@
         def _():
             kv_arrive(4, 0)
             kv_arrive(4, 1)
+            for k in ks(2):
+                wu_mid(k)
 
         @pl.when(idx == 3)
         def _():
@@ -421,11 +423,14 @@
             for k in ks(1):
                 wu_finish(k)
 
+        @pl.when(idx == 6)
+        def _():
+            for k in ks(2):
+                wu_finish(k)
+
         @pl.when(idx == 7)
         def _():
             wg_step(0, 2)
-            for k in ks(2):
-                wu_mid(k)
 
         return carry
 
@@ -473,10 +478,8 @@
         heads_y(i, y).start()
 
     wg_step(0, 3)
-    for k in ks(2):
-        wu_finish(k)
+    wu_mid(3)
     wg_step(1, 3)
-    wu_mid(3)
     wg_step(2, 3)
     wg_step(3, 3)
     wu_mid(6)

time: 79.8 us -> 79.1 us (level)
  no operation moved by 1% of the time
where the time goes in v5:
time: 79.1 us; the launch traced here: 78.9 us
  Pallas kernels  77.3 us (98%)
  local copies, waits for them, and re-layouts  1.62 us (2%)
    pallas_call x1, Pallas kernels, layer(): pl.pallas_call(layer_kernel, out_shape=jax.ShapeDtypeStruct((ROWS // NY,...  77.3 us
    unnamed x1, local copies, waits for them, and re-layouts  1.62 us

profile of v5, /device:TPU:8, one launch (start us, length us, event | category | flops | bytes accessed | tf_op | source)
XLA Modules:
  0.0 78.9 jit_solution(2311670500239523018)
XLA Ops:
  0.0 77.3 %layer.1 = bf16[48,2048]{1,0:T(8,128)(2,1)} custom-call(bf16[192,128]{1,0:T(8,128)(2,1)} %qa.1, bf16[192,128]{1,0:T(8,128)(2,1)} %qb.1, bf16[192,128]{1,0:T(8,128)(2,1)} %ka.1, bf16[192,128]{1,0:T(8,128)(2,1)} %kb.1, bf16[192,256]{1,0:T(8,128)(2,1)} %va.1, bf16[32,1408]{1,0:T(8,128)(2,1)} %gw.1, bf16[32,1408]{1,0:T(8,128)(2,1)} %uw.1, ...), custom_call_target="tpu_custom_call" | custom-call | tf_op jit(solution)/shard_map/layer/pallas_call | solution.py:607
  77.3 1.6 %copy.17 = bf16[48,2048]{1,0:T(8,128)(2,1)} copy(bf16[48,2048]{1,0:T(8,128)(2,1)} %layer.1) | data formatting | bytes 393216

commit v6 on v5

--- a/solution.py
+++ b/solution.py
@@ -602,7 +602,7 @@
     SM = pl.BlockSpec(memory_space=pltpu.SMEM)
     ff, width = args[5].shape[1], args[8].shape[1]
     dma = pltpu.SemaphoreType.DMA
-    cut = 9 * 128 if ff > 9 * 128 else ff // 2
+    cut = 8 * 128 if ff > 8 * 128 else ff // 2
     sems = [(11,), (17,), (8,), (3,), (2, 2, 4), (8,), (2, 4), (8, 2), (8,), (NX, 2, 4), (8,), (NY,)]
     return pl.pallas_call(
         layer_kernel,

time: 79.1 us -> 78.8 us (level)
  no operation moved by 1% of the time
where the time goes in v6:
time: 78.8 us; the launch traced here: 78.7 us
  Pallas kernels  77.1 us (98%)
  local copies, waits for them, and re-layouts  1.62 us (2%)
    pallas_call x1, Pallas kernels, layer(): pl.pallas_call(layer_kernel, out_shape=jax.ShapeDtypeStruct((ROWS // NY,...  77.1 us
    unnamed x1, local copies, waits for them, and re-layouts  1.62 us

profile of v6, /device:TPU:8, one launch (start us, length us, event | category | flops | bytes accessed | tf_op | source)
XLA Modules:
  0.0 78.7 jit_solution(10882649905236109594)
XLA Ops:
  0.0 77.1 %layer.1 = bf16[48,2048]{1,0:T(8,128)(2,1)} custom-call(bf16[192,128]{1,0:T(8,128)(2,1)} %qa.1, bf16[192,128]{1,0:T(8,128)(2,1)} %qb.1, bf16[192,128]{1,0:T(8,128)(2,1)} %ka.1, bf16[192,128]{1,0:T(8,128)(2,1)} %kb.1, bf16[192,256]{1,0:T(8,128)(2,1)} %va.1, bf16[32,1408]{1,0:T(8,128)(2,1)} %gw.1, bf16[32,1408]{1,0:T(8,128)(2,1)} %uw.1, ...), custom_call_target="tpu_custom_call" | custom-call | tf_op jit(solution)/shard_map/layer/pallas_call | solution.py:607
  77.1 1.6 %copy.17 = bf16[48,2048]{1,0:T(8,128)(2,1)} copy(bf16[48,2048]{1,0:T(8,128)(2,1)} %layer.1) | data formatting | bytes 393216

commit v7 on v6

--- a/solution.py
+++ b/solution.py
@@ -502,6 +502,7 @@
             else:
                 more = more + stream[:, :, cols]
             stream[:, :, cols] = more
+    wu_mid(7)
     rows = stream[...].reshape(ROWS, width)
     normed = rms_scale(rows, mix_gain[...]).astype(bf16)
     for zz in range(NZ):
@@ -513,7 +514,6 @@
         two = order[n : n + 2]
         if n == 0:
             wg_step(0, 4)
-            wu_mid(7)
         if n == 2:
             wg_step(1, 4)
             wg_step(2, 4)

time: 78.8 us -> 78.6 us (level)
  no operation moved by 1% of the time
where the time goes in v7:
time: 78.6 us; the launch traced here: 78.5 us
  Pallas kernels  76.9 us (98%)
  local copies, waits for them, and re-layouts  1.62 us (2%)
    pallas_call x1, Pallas kernels, layer(): pl.pallas_call(layer_kernel, out_shape=jax.ShapeDtypeStruct((ROWS // NY,...  76.9 us
    unnamed x1, local copies, waits for them, and re-layouts  1.62 us

profile of v7, /device:TPU:8, one launch (start us, length us, event | category | flops | bytes accessed | tf_op | source)
XLA Modules:
  0.0 78.5 jit_solution(15009728311244829991)
XLA Ops:
  0.0 76.9 %layer.1 = bf16[48,2048]{1,0:T(8,128)(2,1)} custom-call(bf16[192,128]{1,0:T(8,128)(2,1)} %qa.1, bf16[192,128]{1,0:T(8,128)(2,1)} %qb.1, bf16[192,128]{1,0:T(8,128)(2,1)} %ka.1, bf16[192,128]{1,0:T(8,128)(2,1)} %kb.1, bf16[192,256]{1,0:T(8,128)(2,1)} %va.1, bf16[32,1408]{1,0:T(8,128)(2,1)} %gw.1, bf16[32,1408]{1,0:T(8,128)(2,1)} %uw.1, ...), custom_call_target="tpu_custom_call" | custom-call | tf_op jit(solution)/shard_map/layer/pallas_call | solution.py:607
  76.9 1.6 %copy.17 = bf16[48,2048]{1,0:T(8,128)(2,1)} copy(bf16[48,2048]{1,0:T(8,128)(2,1)} %layer.1) | data formatting | bytes 393216
